TPU v7x, 32 devices: a whole 2x2x4 slice. The times are simulated.
32 devices in a mesh: ep: 8 (over z, y), tp: 4 (over x, core).
Axes of the slice: x: 2, y: 2, z: 4, core: 2. Of those that a mesh axis runs over, the one named last changes fastest.
Arguments:
- query_latent: bfloat16 [1024, 768], P('ep'), may hold values from -6 to 6
- keyval_latent: bfloat16 [1024, 512], P('ep'), may hold values from -6 to 6
- rotary_key: bfloat16 [1024, 32], P('ep'), may hold values from -6 to 6
- query_gain: float32 [768], replicated, may hold values from 0.3 to 48
- keyval_gain: float32 [512], replicated, may hold values from 0.1 to 1.9
- query_weight: bfloat16 [768, 1536], P(None, 'tp'), may hold values from -0.21875 to 0.21875
- keyval_weight: bfloat16 [512, 2048], P(None, 'tp'), may hold values from -0.25 to 0.25
- output_weight: bfloat16 [1024, 2048], P('tp'), may hold values from -0.1875 to 0.1875
- output_gain: float32 [2048], replicated, may hold values from 0.1 to 1.9
- second_rows: bfloat16 [1024, 2048], P('ep'), may hold values from -6 to 6
- second_gain: float32 [2048], replicated, may hold values from 0.1 to 1.9
- route_ids: int32 [1024, 4], P('ep'), may hold values from 0 to 7, all different within a row; in each aligned block of 128 rows (0 to 127, 128 to 255, ...) at most 128 rows name the same one
- route_weights: float32 [1024, 4], P('ep'), may hold values from 0.1 to 1
- gate_weight: bfloat16 [8, 2048, 1024], P('ep', None, 'tp'), may hold values from -0.125 to 0.125
- up_weight: bfloat16 [8, 2048, 1024], P('ep', None, 'tp'), may hold values from -0.125 to 0.125
- down_weight: bfloat16 [8, 1024, 2048], P('ep', 'tp'), may hold values from -0.1875 to 0.1875
- shared_gate: bfloat16 [2048, 512], P(None, 'tp'), may hold values from -0.125 to 0.125
- shared_up: bfloat16 [2048, 512], P(None, 'tp'), may hold values from -0.125 to 0.125
- shared_down: bfloat16 [512, 2048], P('tp'), may hold values from -0.25 to 0.25
Outputs:
- mixed: bfloat16 [1024, 2048], P(('ep', 'tp'))
- expert_mix: bfloat16 [1024, 2048], P('ep', 'tp')
Inputs may be any that keep to these rules, and one draw needn't show every extreme that they name: `route_ids`: each row names 4 different experts. Among the rows of one index of ep (aligned blocks of 128 rows) no expert is named more than 128 times, a bound that some expert reaches in some blocks.
All inputs are finite; a program needn't handle non-finite values.
Results may differ from a plain program's by a relative error of at most 0.023.
The roundings to bfloat16 on the way count: a program that leaves them out, or rounds other values in their place, can miss the bound.
Values may be sent and summed in bfloat16 or wider, within the bound.
A program may use at most 128 MiB of HBM per device.

v0:
```python
import math

import jax
import jax.numpy as jnp
from jax import lax
from jax.sharding import PartitionSpec as P

NOPE = 64
ROPE = 32
VDIM = 64


EPS = 1e-06
ROPE_BASE = 10000.0


def rms_scale(values, gain_vec):
    widened = values.astype(jnp.float32)
    normed = widened * lax.rsqrt(jnp.mean(widened * widened, -1, keepdims=True) + EPS)
    return (normed * gain_vec).astype(jnp.bfloat16)


def rotate(values, positions):
    half_width = values.shape[-1] // 2
    inverse = 1.0 / ROPE_BASE ** (
        jnp.arange(half_width, dtype=jnp.float32) * 2.0 / (2 * half_width)
    )
    angles = positions[:, None] * inverse[None, :]
    cosine = jnp.cos(angles)
    sine_vals = jnp.sin(angles)
    if values.ndim == 3:
        cosine = cosine[:, None, :]
        sine_vals = sine_vals[:, None, :]
    first_half = values[..., :half_width]
    second = values[..., half_width:]
    return jnp.concatenate(
        [first_half * cosine - second * sine_vals, first_half * sine_vals + second * cosine], -1
    )


def per_device(
    query_latent,
    keyval_latent,
    rotary_key,
    query_gain,
    keyval_gain,
    query_weight,
    keyval_weight,
    output_weight,
    output_gain,
    second_rows,
    second_gain,
    route_ids,
    route_weights,
    gate_weight,
    up_weight,
    down_weight,
    shared_gate,
    shared_up,
    shared_down,
):
    first_rows = query_latent.shape[0]
    tp_count = lax.axis_size("tp")
    ep_count = lax.axis_size("ep")
    head_count = query_weight.shape[1] // (NOPE + ROPE)
    positions = (lax.axis_index("ep") * first_rows).astype(jnp.float32) + jnp.arange(
        first_rows, dtype=jnp.float32
    )
    queries = jnp.dot(
        rms_scale(query_latent, query_gain), query_weight, preferred_element_type=jnp.float32
    ).reshape(first_rows, head_count, NOPE + ROPE)
    queries = jnp.concatenate(
        [queries[..., :NOPE], rotate(queries[..., NOPE:], positions)], -1
    ).astype(jnp.bfloat16)
    query_plain = queries[..., :NOPE]
    query_turned = queries[..., NOPE:]
    kv_normed = rms_scale(keyval_latent, keyval_gain)
    key_rot = rotate(rotary_key.astype(jnp.float32), positions).astype(jnp.bfloat16)
    score_scale = (NOPE + ROPE) ** (-0.5)

    def attend(carried, pieces):
        highest, denominator, accumulated = carried
        keyval_piece, rot_piece = pieces
        key_count = keyval_piece.shape[0]
        keyval_heads = keyval_piece.reshape(key_count, head_count, NOPE + VDIM)
        scores = jnp.einsum(
            "qhd,khd->hqk",
            query_plain,
            keyval_heads[..., :NOPE],
            preferred_element_type=jnp.float32,
        )
        scores = (
            scores
            + jnp.einsum("qhr,kr->hqk", query_turned, rot_piece, preferred_element_type=jnp.float32)
        ) * score_scale
        new_high = jnp.maximum(highest, jnp.max(scores, -1))
        exponent = jnp.exp(scores - new_high[..., None])
        rescale = jnp.exp(highest - new_high)
        denominator = denominator * rescale + jnp.sum(exponent, -1)
        update = jnp.einsum(
            "hqk,khe->qhe",
            exponent.astype(jnp.bfloat16),
            keyval_heads[..., NOPE:],
            preferred_element_type=jnp.float32,
        )
        accumulated = accumulated * rescale.T[..., None] + update
        return (new_high, denominator, accumulated)

    start_state = (
        jnp.full((head_count, first_rows), -jnp.inf, jnp.float32),
        jnp.zeros((head_count, first_rows), jnp.float32),
        jnp.zeros((first_rows, head_count, VDIM), jnp.float32),
    )
    quarter = first_rows // tp_count
    offset = lax.axis_index("tp") * quarter
    own_latent = lax.dynamic_slice_in_dim(kv_normed, offset, quarter, 0)
    own_rot = lax.dynamic_slice_in_dim(key_rot, offset, quarter, 0)
    all_latent, all_rot = (
        lax.all_gather(own_latent, ("ep", "tp"), axis=0, tiled=True),
        lax.all_gather(own_rot, ("ep", "tp"), axis=0, tiled=True),
    )
    total_keys = all_latent.shape[0]
    key_block = math.gcd(total_keys, 512)
    latent_blocks = all_latent.reshape(total_keys // key_block, key_block, all_latent.shape[1])
    rot_blocks = all_rot.reshape(total_keys // key_block, key_block, all_rot.shape[1])

    def scan_step(carried, block_pair):
        projected = jnp.dot(
            block_pair[0], keyval_weight, preferred_element_type=jnp.float32
        ).astype(jnp.bfloat16)
        return (attend(carried, (projected, block_pair[1])), None)

    final_state, _ = lax.scan(scan_step, start_state, (latent_blocks, rot_blocks))
    denominator = final_state[1]
    accumulated = final_state[2]
    attended = (
        (accumulated / denominator.T[..., None])
        .astype(jnp.bfloat16)
        .reshape(first_rows, head_count * VDIM)
    )
    mixture = lax.psum_scatter(
        jnp.dot(attended, output_weight, preferred_element_type=jnp.float32).astype(jnp.bfloat16),
        "tp",
        scatter_dimension=0,
        tiled=True,
    ).astype(jnp.float32)
    mixed = rms_scale(mixture, output_gain)
    tok_rows = second_rows.shape[0]
    model_width = second_rows.shape[1]
    top_count = route_ids.shape[1]
    local_count = gate_weight.shape[0]
    expert_count = local_count * ep_count
    capacity = max(tp_count, tok_rows * top_count * 2 // expert_count // tp_count * tp_count)
    normed = rms_scale(second_rows, second_gain)
    flat_ids = route_ids.reshape(-1)
    onehot = (flat_ids[:, None] == jnp.arange(expert_count, dtype=jnp.int32)[None, :]).astype(
        jnp.int32
    )
    slot_rank = jnp.sum((jnp.cumsum(onehot, 0) - 1) * onehot, 1)
    owners = jnp.arange(tok_rows * top_count, dtype=jnp.int32) // top_count
    slot_table = (
        jnp.full((expert_count * capacity,), tok_rows, jnp.int32)
        .at[flat_ids * capacity + slot_rank]
        .set(owners)
    )
    padded = jnp.concatenate([normed, jnp.zeros((1, model_width), jnp.bfloat16)], 0)
    outgoing = padded[slot_table].reshape(ep_count, local_count, capacity, model_width)
    weights = route_weights.reshape(-1, 1)
    shared_hidden = (
        jax.nn.silu(jnp.dot(normed, shared_gate, preferred_element_type=jnp.float32))
        * jnp.dot(normed, shared_up, preferred_element_type=jnp.float32)
    ).astype(jnp.bfloat16)
    shared_part = jnp.dot(shared_hidden, shared_down, preferred_element_type=jnp.float32)
    arrived = lax.all_to_all(outgoing, "ep", split_axis=0, concat_axis=0, tiled=True)
    gate_act = jnp.einsum(
        "sicd,idf->sicf", arrived, gate_weight, preferred_element_type=jnp.float32
    )
    up_act = jnp.einsum("sicd,idf->sicf", arrived, up_weight, preferred_element_type=jnp.float32)
    hidden = (jax.nn.silu(gate_act) * up_act).astype(jnp.bfloat16)
    slot_terms = jnp.einsum(
        "sicf,ifd->sicd", hidden, down_weight, preferred_element_type=jnp.float32
    ).reshape(-1, model_width)
    slot_sum, shared_sum = (
        lax.psum_scatter(
            slot_terms.astype(jnp.bfloat16), "tp", scatter_dimension=1, tiled=True
        ).astype(jnp.float32),
        lax.psum_scatter(
            shared_part.astype(jnp.bfloat16), "tp", scatter_dimension=1, tiled=True
        ).astype(jnp.float32),
    )
    column_part = model_width // tp_count
    returned = lax.all_to_all(
        slot_sum.astype(jnp.bfloat16).reshape(ep_count, local_count * capacity, column_part),
        "ep",
        split_axis=0,
        concat_axis=0,
        tiled=True,
    )
    returned = returned.reshape(expert_count * capacity, column_part)
    picked = returned[flat_ids * capacity + slot_rank].astype(jnp.float32) * weights
    routed = jnp.sum(picked.reshape(tok_rows, top_count, column_part), 1)
    expert_mix = (routed + shared_sum).astype(jnp.bfloat16)
    return (mixed, expert_mix)


def solution(mesh):
    placed = (
        P("ep", None),
        P("ep", None),
        P("ep", None),
        P(),
        P(),
        P(None, "tp"),
        P(None, "tp"),
        P("tp", None),
        P(),
        P("ep", None),
        P(),
        P("ep", None),
        P("ep", None),
        P("ep", None, "tp"),
        P("ep", None, "tp"),
        P("ep", "tp", None),
        P(None, "tp"),
        P(None, "tp"),
        P("tp", None),
    )
    return jax.shard_map(
        per_device,
        mesh=mesh,
        in_specs=placed,
        out_specs=(P(("ep", "tp"), None), P("ep", "tp")),
        check_vma=False,
    )
```

profile of v0, /device:TPU:0, one launch (start us, length us, event | category | flops | bytes accessed | tf_op | source)
XLA Modules:
  0.0 243.5 jit_solution(6417389296293374427)
XLA Ops:
  8.0 0.8 broadcast_multiply_fusion
  8.8 0.8 copy.51
  9.6 0.1 eq.29
  9.7 0.1 eq.25
  9.8 1.2 fusion.39
  11.0 0.1 copy.50
  11.2 0.1 mul.242
  11.3 1.1 reduce-window.6
  12.4 0.2 slice_reduce_fusion
  12.7 0.1 fusion.70
  12.8 2.4 %scatter_custom_fusion = s32[1024]{0:T(1024)S(1)} fusion(s32[512]{0:T(512)S(1)} %bitcast.145, s32[512]{0:T(512)S(1)} %add_select_fusion, s32[]{:T(128)} %constant.51.clone.1), kind=kCustom, calls=%fused_computation.107 | custom fusion | bytes 4100 | tf_op jit(solution)/shard_map/scatter | solution.py:164
  15.3 1.2 fusion.41
  16.5 6.0 %gather_fusion = bf16[1024,2048]{1,0:T(8,128)(2,1)} fusion(bf16[129,2048]{1,0:T(8,128)(2,1)S(1)} %concatenate.14, s32[1024]{0:T(1024)S(1)} %fusion.72), kind=kCustom, calls=%fused_computation | custom fusion | bytes 8392704 | tf_op jit(solution)/shard_map/gather | solution.py:167
  22.6 7.4 %all-to-all-start = ((bf16[8,1,128,2048]{3,2,1,0:T(8,128)(2,1)}), bf16[8,1,128,2048]{3,2,1,0:T(8,128)(2,1)}, u32[]{:S(2)}, u32[]{:S(2)}) async-start(bf16[8,1,128,2048]{3,2,1,0:T(8,128)(2,1)} %bitcast.136), calls=%async_computation.1 | async-start | bytes 8388608 | tf_op jit(solution)/shard_map/all_to_all | solution.py:174
  30.0 0.0 all-gather.2.cloned.1.call-start
  30.1 0.1 multiply_reduce_fusion.1
  30.2 0.1 dynamic-slice
  30.3 0.7 fusion.63
  31.0 0.0 all-gather.2.cloned.1.call-update
  31.0 0.0 reduce-scatter.6.cloned.1.call-start
  31.1 97.0 %all-to-all-done = bf16[8,1,128,2048]{3,2,1,0:T(8,128)(2,1)} async-done(((bf16[8,1,128,2048]{3,2,1,0:T(8,128)(2,1)}), bf16[8,1,128,2048]{3,2,1,0:T(8,128)(2,1)}, u32[]{:S(2)}, u32[]{:S(2)}) %all-to-all-start) | async-done | bytes 4194336 | tf_op jit(solution)/shard_map/all_to_all | solution.py:174
  128.1 4.5 %fusion.21 = f32[8,1,128,256]{3,2,0,1:T(8,128)} fusion(bf16[8,1,128,2048]{3,2,1,0:T(8,128)(2,1)} %all-to-all-done, bf16[1,2048,256]{2,1,0:T(8,128)(2,1)S(1)} %copy-done.11), kind=kOutput, calls=%fused_computation.35 | convolution fusion | flops 1073741824 | bytes 6291456 | tf_op jit(solution)/shard_map/sicd,idf->sicf/dot_general | solution.py:175
  132.6 9.1 %convolution_convert_fusion.1 = bf16[8,128,2048]{2,1,0:T(8,128)(2,1)} fusion(bf16[8,1,128,2048]{3,2,1,0:T(8,128)(2,1)} %all-to-all-done, bf16[1,256,2048]{2,1,0:T(8,128)(2,1)S(1)} %copy-done, bf16[1,2048,256]{2,1,0:T(8,128)(2,1)} %param.35, f32[8,1,128,256]{3,2,0,1:T(8,128)} %fusion.21), kind=kOutput, calls=%fused_computation.32 | convolution fusion | flops 2151153664 | bytes 11534336 | tf_op jit(solution)/shard_map/sicf,ifd->sicd/dot_general | solution.py:180
  141.6 0.0 reduce-scatter.6.cloned.1.call-update
  141.7 0.0 reduce-scatter.4.cloned.1.call-start
  141.7 0.6 copy-done.6
  142.3 0.1 multiply_cosine_fusion
  142.5 0.1 dynamic-slice_maximum_fusion
  142.5 0.1 copy.59
  142.6 0.1 fusion.52
  142.8 0.0 copy-done.4
  142.8 0.4 fusion.58
  143.2 40.9 %all_gather.7 = bf16[1024,32]{1,0:T(8,128)(2,1)S(1)} all-gather(bf16[32,32]{1,0:T(8,128)(2,1)S(1)} %copy.59), channel_id=1, replica_groups=mesh['ep'=8,'tp'=4] {'ep','tp'}, dimensions={0}, use_global_device_ids=true | all-gather | bytes 67584 | tf_op jit(solution)/shard_map/all_gather | solution.py:120
  184.1 0.1 copy.49
  184.3 0.0 all-gather.2.cloned.1.call-done
  184.3 5.6 %while.15 = (s32[]{:T(128)}, f32[4,128]{1,0:T(4,128)S(1)}, f32[4,128]{1,0:T(4,128)S(1)}, f32[128,4,64]{0,2,1:T(8,128)S(1)}, bf16[2,512,512]{2,1,0:T(8,128)(2,1)}...) while((s32[]{:T(128)}, f32[4,128]{1,0:T(4,128)S(1)}, ...), condition=%wide.region_5.6_spmd.clone, body=%wide.region_2.5_spmd.clone.sunk | while | flops 354520064 | bytes 7766153 | solution.py:133
  184.3 1.6 convolution_convert_fusion.5
  186.0 0.3 convolution_bitcast_fusion.4
  186.3 0.3 fusion.112
  186.7 0.3 fusion.116
  187.0 0.2 fusion.114
  187.2 1.5 convolution_convert_fusion.5
  188.7 0.3 convolution_bitcast_fusion.4
  189.1 0.3 fusion.112
  189.4 0.3 fusion.116
  189.8 0.2 fusion.114
  190.0 1.1 convolution_convert_fusion.3
  191.2 0.0 reduce-scatter.4.cloned.1.call-update
  191.2 0.0 reduce-scatter.6.cloned.1.call-done
  191.2 3.6 %all-to-all-start.1 = ((bf16[8,128,512]{2,1,0:T(8,128)(2,1)}), bf16[8,128,512]{2,1,0:T(8,128)(2,1)S(1)}, u32[]{:S(2)}, u32[]{:S(2)}) async-start(bf16[8,128,512]{2,1,0:T(8,128)(2,1)} %bitcast.140), calls=%async_computation.3 | async-start | bytes 2097152 | tf_op jit(solution)/shard_map/all_to_all | solution.py:192
  194.8 0.2 reduce-scatter.8.cloned.1.call-start
  195.0 1.3 fusion.81
  196.4 2.5 %convolution_convert_fusion.2 = bf16[128,2048]{1,0:T(8,128)(2,1)} fusion(bf16[128,2048]{1,0:T(8,128)(2,1)} %param.39, bf16[128,2048]{1,0:T(8,128)(2,1)S(1)} %fusion.41, bf16[2048,128]{1,0:T(8,128)(2,1)} %param.38, f32[128,128]{1,0:T(8,128)S(1)} %fusion.81), kind=kOutput, calls=%fused_computation.33 | convolution fusion | flops 134578176 | bytes 2162688 | tf_op jit(solution)/shard_map/dot_general | solution.py:173
  198.9 0.0 reduce-scatter.8.cloned.1.call-update
  198.9 0.1 copy.54
  199.1 11.2 %reduce-scatter.4.cloned.1.call-done = bf16[32,2048]{1,0:T(8,128)(2,1)} async-done(((bf16[128,2048]{1,0:T(8,128)(2,1)}), bf16[32,2048]{1,0:T(8,128)(2,1)}) %reduce-scatter.4.cloned.1.call-update) | async-done | bytes 131088 | tf_op jit(solution)/shard_map/reduce_scatter | solution.py:141
  210.3 1.0 fusion.55
  211.4 1.7 fusion.57
  213.0 8.2 %all-to-all-done.1 = bf16[8,128,512]{2,1,0:T(8,128)(2,1)S(1)} async-done(((bf16[8,128,512]{2,1,0:T(8,128)(2,1)}), bf16[8,128,512]{2,1,0:T(8,128)(2,1)S(1)}, u32[]{:S(2)}, u32[]{:S(2)}) %all-to-all-start.1) | async-done | bytes 1048608 | tf_op jit(solution)/shard_map/all_to_all | solution.py:192
  221.3 2.0 gather_fusion.1
  223.2 0.3 reshape.218
  223.6 0.7 multiply_reduce_fusion
  224.3 10.0 %reduce-scatter.8.cloned.1.call-done = bf16[128,512]{1,0:T(8,128)(2,1)} async-done(((bf16[128,2048]{1,0:T(8,128)(2,1)}), bf16[128,512]{1,0:T(8,128)(2,1)}) %reduce-scatter.8.cloned.1.call-update) | async-done | bytes 131088 | tf_op jit(solution)/shard_map/reduce_scatter | solution.py:187
  234.3 1.6 add_convert_fusion
  (51 shorter events, 0.4 us)
Async XLA Ops:
  8.0 124.6 %copy-start = (bf16[1,256,2048]{2,1,0:T(8,128)(2,1)S(1)}, bf16[1,256,2048]{2,1,0:T(8,128)(2,1)}, u32[]{:S(2)}) copy-start(bf16[1,256,2048]{2,1,0:T(8,128)(2,1)} %param.36) | copy-start | bytes 3145732
  22.6 7.5 %copy-start.5 = (bf16[128,512]{1,0:T(8,128)(2,1)S(1)}, bf16[128,512]{1,0:T(8,128)(2,1)}, u32[]{:S(2)}) copy-start(bf16[128,512]{1,0:T(8,128)(2,1)} %param.22) | copy-start | bytes 393220
  22.6 7.7 %copy-start.9 = (f32[512]{0:T(512)S(1)}, f32[512]{0:T(512)}, u32[]{:S(2)}) copy-start(f32[512]{0:T(512)} %param.25) | copy-start | bytes 6148
  22.6 105.5 %copy-start.11 = (bf16[1,2048,256]{2,1,0:T(8,128)(2,1)S(1)}, bf16[1,2048,256]{2,1,0:T(8,128)(2,1)}, u32[]{:S(2)}) copy-start(bf16[1,2048,256]{2,1,0:T(8,128)(2,1)} %param.34) | copy-start | bytes 3145732
  22.6 105.5 %all-to-all-start = ((bf16[8,1,128,2048]{3,2,1,0:T(8,128)(2,1)}), bf16[8,1,128,2048]{3,2,1,0:T(8,128)(2,1)}, u32[]{:S(2)}, u32[]{:S(2)}) async-start(bf16[8,1,128,2048]{3,2,1,0:T(8,128)(2,1)} %bitcast.136), calls=%async_computation.1 | async-start | bytes 8388608 | tf_op jit(solution)/shard_map/all_to_all | solution.py:174
  30.0 154.3 %all-gather.2.cloned.1.call-start = ((), (), s32[]{:S(2)}) async-start(), calls=%async_computation.5 | async-start | bytes 1081344 | tf_op jit(solution)/shard_map/all_gather | solution.py:119
  31.0 160.2 %reduce-scatter.6.cloned.1.call-start = ((), (), s32[]{:S(2)}) async-start(), calls=%async_computation.7 | async-start | bytes 5242880 | tf_op jit(solution)/shard_map/reduce_scatter | solution.py:184
  141.6 0.7 copy-start.6
  141.6 1.0 copy-start.3
  141.6 1.2 copy-start.4
  141.6 1.2 copy-start.8
  141.6 42.7 %copy-start.1 = (bf16[512,512]{1,0:T(8,128)(2,1)S(1)}, bf16[512,512]{1,0:T(8,128)(2,1)}, u32[]{:S(2)}) copy-start(bf16[512,512]{1,0:T(8,128)(2,1)} %param.27) | copy-start | bytes 1572868
  141.7 68.6 %reduce-scatter.4.cloned.1.call-start = ((), (), s32[]{:S(2)}) async-start(), calls=%async_computation.6 | async-start | bytes 655360 | tf_op jit(solution)/shard_map/reduce_scatter | solution.py:141
  184.3 5.7 %copy-start.2 = (bf16[256,2048]{1,0:T(8,128)(2,1)S(1)}, bf16[256,2048]{1,0:T(8,128)(2,1)}, u32[]{:S(2)}) copy-start(bf16[256,2048]{1,0:T(8,128)(2,1)} %param.28) | copy-start | bytes 3145732
  190.0 9.0 %copy-start.10 = (f32[128,4]{0,1:T(4,128)S(1)}, f32[128,4]{0,1:T(4,128)}, u32[]{:S(2)}) copy-start(f32[128,4]{0,1:T(4,128)} %param.33) | copy-start | bytes 6148
  190.0 21.4 %copy-start.7 = (f32[2048]{0:T(1024)S(1)}, f32[2048]{0:T(1024)}, u32[]{:S(2)}) copy-start(f32[2048]{0:T(1024)} %param.29) | copy-start | bytes 24580
  191.2 30.0 %all-to-all-start.1 = ((bf16[8,128,512]{2,1,0:T(8,128)(2,1)}), bf16[8,128,512]{2,1,0:T(8,128)(2,1)S(1)}, u32[]{:S(2)}, u32[]{:S(2)}) async-start(bf16[8,128,512]{2,1,0:T(8,128)(2,1)} %bitcast.140), calls=%async_computation.3 | async-start | bytes 2097152 | tf_op jit(solution)/shard_map/all_to_all | solution.py:192
  194.8 39.5 %reduce-scatter.8.cloned.1.call-start = ((), (), s32[]{:S(2)}) async-start(), calls=%async_computation.8 | async-start | bytes 655360 | tf_op jit(solution)/shard_map/reduce_scatter | solution.py:187
Sparse Core Ops, SparseCore 0:
  34.3 96.0 all-gather.1
Sparse Core Ops, SparseCore 1:
  141.7 44.8 reduce-scatter.5
  191.3 19.0 reduce-scatter.3
  212.7 21.6 reduce-scatter.7
where the time goes:
time: 244 us; the launch traced here: 243 us
  waiting for transfers between devices  127 us (52%)
  blocking collectives  40.9 us (17%)
  matrix products  24.1 us (10%)
  between operations  16 us (7%)
  local copies, waits for them, and re-layouts  13.3 us (5%)
  starting transfers between devices  11.4 us (5%)
  other arithmetic  11.1 us (5%)
    all_to_all x1, waiting for transfers between devices, per_device(): lax.all_to_all(outgoing, 'ep', split_axis=0, concat_axis=0, tiled=True)  97 us
    all_gather x1, blocking collectives, per_device(): lax.all_gather(own_rot, ('ep', 'tp'), axis=0, tiled=True)  40.9 us
    reduce_scatter x1, waiting for transfers between devices, per_device(): lax.psum_scatter(jnp.dot(attended, output_weight, preferred_element_type=...  11.2 us
    reduce_scatter x1, waiting for transfers between devices, per_device(): lax.psum_scatter(shared_part.astype(jnp.bfloat16), 'tp', scatter_dimensio...  10 us
    dot_general x1, matrix products, per_device(): jnp.einsum('sicf,ifd->sicd', hidden, down_weight, preferred_element_type=...  9.05 us
    all_to_all x1, waiting for transfers between devices, per_device(): lax.all_to_all(slot_sum.astype(jnp.bfloat16).reshape(ep_count, local_coun...  8.24 us
    all_to_all x1, starting transfers between devices, per_device(): lax.all_to_all(outgoing, 'ep', split_axis=0, concat_axis=0, tiled=True)  7.45 us
    gather x1, local copies, waits for them, and re-layouts, per_device(): padded[slot_table].reshape(ep_count, local_count, capacity, model_width)  6.02 us
  transfers between devices with their start and end apart: 6, of which 4 were waited for; matrix products, arithmetic and copies ran while one was open for 13% of the time, Pallas kernels for 0%

commit v1 on v0

--- a/solution.py
+++ b/solution.py
@@ -1,8 +1,11 @@
+import functools
 import math
 
 import jax
 import jax.numpy as jnp
 from jax import lax
+from jax.experimental import pallas as pl
+from jax.experimental.pallas import tpu as pltpu
 from jax.sharding import PartitionSpec as P
 
 NOPE = 64
@@ -38,7 +41,7 @@
     )
 
 
-def per_device(
+def per_device_slots(
     query_latent,
     keyval_latent,
     rotary_key,
@@ -203,6 +206,225 @@
     return (mixed, expert_mix)
 
 
+def experts_kernel(
+    tp_count,
+    blocks,
+    rows_ref,
+    scale_ref,
+    gate_ref,
+    up_ref,
+    down_ref,
+    shared_gate_ref,
+    shared_up_ref,
+    shared_down_ref,
+    out_ref,
+    total,
+):
+    step = pl.program_id(0)
+    me = lax.axis_index("ep")
+    tile = rows_ref.shape[0]
+    block_rows = tile // blocks
+    width = down_ref.shape[1]
+    part = width // tp_count
+    rows = rows_ref[...]
+    gate_act = jnp.dot(rows, gate_ref[...], preferred_element_type=jnp.float32)
+    up_act = jnp.dot(rows, up_ref[...], preferred_element_type=jnp.float32)
+    hidden = gate_act / (1.0 + jnp.exp(-gate_act)) * up_act * scale_ref[...]
+    total[...] = jnp.dot(
+        hidden.astype(jnp.bfloat16), down_ref[...], preferred_element_type=jnp.float32
+    )
+
+    for block in range(blocks):
+
+        @pl.when(step * blocks + block == me)
+        def _():
+            span = pl.ds(block * block_rows, block_rows)
+            own = rows_ref[span, :]
+            gate_own = jnp.dot(own, shared_gate_ref[...], preferred_element_type=jnp.float32)
+            up_own = jnp.dot(own, shared_up_ref[...], preferred_element_type=jnp.float32)
+            hidden_own = gate_own / (1.0 + jnp.exp(-gate_own)) * up_own
+            total[span, :] += jnp.dot(
+                hidden_own.astype(jnp.bfloat16),
+                shared_down_ref[...],
+                preferred_element_type=jnp.float32,
+            )
+
+    for block in range(blocks):
+        for column in range(tp_count):
+            out_ref[pl.ds((block * tp_count + column) * block_rows, block_rows), :] = total[
+                block * block_rows : (block + 1) * block_rows, column * part : (column + 1) * part
+            ].astype(jnp.bfloat16)
+
+
+def run_experts(rows, scale, gate, up, down, shared_gate, shared_up, shared_down, ep_count, tp_count):
+    count, width = rows.shape
+    block_rows = count // ep_count
+    blocks = math.gcd(ep_count, 2)
+    tile = block_rows * blocks
+    part = width // tp_count
+
+    def whole(array):
+        return pl.BlockSpec(array.shape, lambda i: (0, 0))
+
+    return pl.pallas_call(
+        functools.partial(experts_kernel, tp_count, blocks),
+        out_shape=jax.ShapeDtypeStruct((count * tp_count, part), jnp.bfloat16),
+        grid=(count // tile,),
+        in_specs=[
+            pl.BlockSpec((tile, width), lambda i: (i, 0)),
+            pl.BlockSpec((tile, 1), lambda i: (i, 0)),
+            whole(gate),
+            whole(up),
+            whole(down),
+            whole(shared_gate),
+            whole(shared_up),
+            whole(shared_down),
+        ],
+        out_specs=pl.BlockSpec((tile * tp_count, part), lambda i: (i, 0)),
+        scratch_shapes=[pltpu.VMEM((tile, width), jnp.float32)],
+        compiler_params=pltpu.CompilerParams(
+            dimension_semantics=("arbitrary",), vmem_limit_bytes=48 * 1024 * 1024
+        ),
+        cost_estimate=pl.CostEstimate(
+            flops=6 * count * width * gate.shape[1],
+            bytes_accessed=4 * count * width + 6 * width * gate.shape[1],
+            transcendentals=count * gate.shape[1],
+        ),
+    )(rows, scale, gate, up, down, shared_gate, shared_up, shared_down)
+
+
+def per_device_dense(
+    query_latent,
+    keyval_latent,
+    rotary_key,
+    query_gain,
+    keyval_gain,
+    query_weight,
+    keyval_weight,
+    output_weight,
+    output_gain,
+    second_rows,
+    second_gain,
+    route_ids,
+    route_weights,
+    gate_weight,
+    up_weight,
+    down_weight,
+    shared_gate,
+    shared_up,
+    shared_down,
+):
+    first_rows = query_latent.shape[0]
+    tp_count = lax.axis_size("tp")
+    ep_count = lax.axis_size("ep")
+    head_count = query_weight.shape[1] // (NOPE + ROPE)
+    start_row = lax.axis_index("ep") * first_rows
+    quarter = first_rows // tp_count
+    offset = lax.axis_index("tp") * quarter
+    second_quarter = second_rows.shape[0] // tp_count
+    second_offset = lax.axis_index("tp") * second_quarter
+
+    own_latent = rms_scale(
+        lax.dynamic_slice_in_dim(keyval_latent, offset, quarter, 0), keyval_gain
+    )
+    own_positions = (start_row + offset).astype(jnp.float32) + jnp.arange(
+        quarter, dtype=jnp.float32
+    )
+    own_rot = rotate(
+        lax.dynamic_slice_in_dim(rotary_key, offset, quarter, 0).astype(jnp.float32),
+        own_positions,
+    ).astype(jnp.bfloat16)
+    ids = lax.dynamic_slice_in_dim(route_ids, second_offset, second_quarter, 0)
+    wts = lax.dynamic_slice_in_dim(route_weights, second_offset, second_quarter, 0)
+    dense = jnp.sum(
+        jnp.where(
+            ids[:, :, None] == jnp.arange(ep_count, dtype=jnp.int32)[None, None, :],
+            wts[:, :, None],
+            0.0,
+        ),
+        1,
+    )
+    dense_high = dense.astype(jnp.bfloat16)
+    dense_low = (dense - dense_high.astype(jnp.float32)).astype(jnp.bfloat16)
+    latent_width = own_latent.shape[1]
+    used = latent_width + ROPE + 2 * ep_count
+    fill = -used % 128
+    packed = jnp.concatenate(
+        [own_latent, own_rot, dense_high, dense_low, jnp.zeros((quarter, fill), jnp.bfloat16)], 1
+    )
+    packed = lax.all_gather(packed, ("ep", "tp"), axis=0, tiled=True)
+    own_normed = rms_scale(
+        lax.dynamic_slice_in_dim(second_rows, second_offset, second_quarter, 0), second_gain
+    )
+    own_normed, packed = lax.optimization_barrier((own_normed, packed))
+    normed = lax.all_gather(own_normed, ("ep", "tp"), axis=0, tiled=True)
+
+    positions = start_row.astype(jnp.float32) + jnp.arange(first_rows, dtype=jnp.float32)
+    queries = jnp.dot(
+        rms_scale(query_latent, query_gain), query_weight, preferred_element_type=jnp.float32
+    ).reshape(first_rows, head_count, NOPE + ROPE)
+    queries = jnp.concatenate(
+        [queries[..., :NOPE], rotate(queries[..., NOPE:], positions)], -1
+    ).astype(jnp.bfloat16)
+    all_latent = packed[:, :latent_width]
+    all_rot = packed[:, latent_width : latent_width + ROPE]
+    total_keys = packed.shape[0]
+    keyvals = (
+        jnp.dot(all_latent, keyval_weight, preferred_element_type=jnp.float32)
+        .astype(jnp.bfloat16)
+        .reshape(total_keys, head_count, NOPE + VDIM)
+    )
+    keys = jnp.concatenate(
+        [
+            keyvals[..., :NOPE],
+            jnp.broadcast_to(all_rot[:, None, :], (total_keys, head_count, ROPE)),
+        ],
+        -1,
+    )
+    scores = jnp.einsum("qhd,khd->hqk", queries, keys, preferred_element_type=jnp.float32) * (
+        (NOPE + ROPE) ** (-0.5)
+    )
+    exponent = jnp.exp(scores - jnp.max(scores, -1, keepdims=True))
+    denominator = jnp.sum(exponent, -1)
+    accumulated = jnp.einsum(
+        "hqk,khe->qhe",
+        exponent.astype(jnp.bfloat16),
+        keyvals[..., NOPE:],
+        preferred_element_type=jnp.float32,
+    )
+    attended = (
+        (accumulated / denominator.T[..., None])
+        .astype(jnp.bfloat16)
+        .reshape(first_rows, head_count * VDIM)
+    )
+    head_part = jnp.dot(attended, output_weight, preferred_element_type=jnp.float32).astype(
+        jnp.bfloat16
+    )
+    mixture = lax.psum_scatter(head_part, "tp", scatter_dimension=0, tiled=True).astype(
+        jnp.float32
+    )
+    mixed = rms_scale(mixture, output_gain)
+
+    me = lax.axis_index("ep")
+    high = lax.dynamic_slice_in_dim(packed, latent_width + ROPE + me, 1, 1)
+    low = lax.dynamic_slice_in_dim(packed, latent_width + ROPE + ep_count + me, 1, 1)
+    scale = high.astype(jnp.float32) + low.astype(jnp.float32)
+    parts = run_experts(
+        normed,
+        scale,
+        gate_weight[0],
+        up_weight[0],
+        down_weight[0],
+        shared_gate,
+        shared_up,
+        shared_down,
+        ep_count,
+        tp_count,
+    )
+    expert_mix = lax.psum_scatter(parts, ("ep", "tp"), scatter_dimension=0, tiled=True)
+    return (mixed, expert_mix)
+
+
 def solution(mesh):
     placed = (
         P("ep", None),
@@ -225,6 +447,14 @@
         P(None, "tp"),
         P("tp", None),
     )
+    def per_device(*args):
+        tok_rows, top_count = args[11].shape
+        expert_count = args[13].shape[0] * mesh.shape["ep"]
+        capacity = tok_rows * top_count * 2 // expert_count
+        if args[13].shape[0] == 1 and capacity >= tok_rows:
+            return per_device_dense(*args)
+        return per_device_slots(*args)
+
     return jax.shard_map(
         per_device,
         mesh=mesh,

time: 244 us -> 309 us (1.27)
  waiting for transfers between devices: 127 us -> 261 us
  blocking collectives: 40.9 us -> 0 us
  matrix products: 24.1 us -> 5.79 us
  starting transfers between devices: 11.4 us -> 0.16 us
  Pallas kernels: 0 us -> 8.19 us
  local copies, waits for them, and re-layouts: 13.3 us -> 9.24 us
    reduce_scatter x3 -> x2, waiting for transfers between devices: 21.3 us -> 153 us  [the longest x1 143 us: per_device_dense(): lax.psum_scatter(parts, ('ep', 'tp'), scatter_dimension=0, tiled=True)]
    all_gather x1 -> x2, waiting for transfers between devices: 0.02 us -> 108 us  [the longest x1 54.3 us: per_device_dense(): packed = lax.all_gather(packed, ('ep', 'tp'), axis=0, tiled=True)]
    all_to_all x2 -> x0, waiting for transfers between devices: 105 us -> none  [the longest x1 97 us: per_device(): lax.all_to_all(outgoing, 'ep', split_axis=0, concat_axis=0, tiled=True)]
    all_gather x1 -> x0, blocking collectives: 40.9 us -> none  [per_device(): lax.all_gather(own_rot, ('ep', 'tp'), axis=0, tiled=True)]
    dot_general x14 -> x5, matrix products: 24.1 us -> 5.79 us  [the longest x1 1.83 us: per_device_dense(): jnp.dot(all_latent, keyval_weight, preferred_element_type=jnp.float32)]
    all_to_all x2 -> x0, starting transfers between devices: 11 us -> none  [the longest x1 7.45 us: per_device(): lax.all_to_all(outgoing, 'ep', split_axis=0, concat_axis=0, tiled=True)]
    pallas_call x0 -> x1, Pallas kernels: none -> 8.19 us  [run_experts(): pl.pallas_call(functools.partial(experts_kernel, tp_count, blocks), out_s...]
    gather x2 -> x0, local copies, waits for them, and re-layouts: 7.98 us -> none  [the longest x1 6.02 us: per_device(): padded[slot_table].reshape(ep_count, local_count, capacity, model_width)]
  transfers between devices with their start and end apart: 6 -> 4, of which waited for: 4 -> 4; matrix products, arithmetic and copies ran while one was open for 13% -> 5% of each run, Pallas kernels for 0% -> 3%
where the time goes in v1:
time: 309 us
  waiting for transfers between devices  261 us (84%)
  between operations  14 us (5%)
  other arithmetic  10.4 us (3%)
  local copies, waits for them, and re-layouts  9.24 us (3%)
  Pallas kernels  8.19 us (3%)
  matrix products  5.79 us (2%)
    reduce_scatter x1, waiting for transfers between devices, per_device_dense(): lax.psum_scatter(parts, ('ep', 'tp'), scatter_dimension=0, tiled=True)  143 us
    all_gather x1, waiting for transfers between devices, per_device_dense(): packed = lax.all_gather(packed, ('ep', 'tp'), axis=0, tiled=True)  54.3 us
    all_gather x1, waiting for transfers between devices, per_device_dense(): normed = lax.all_gather(own_normed, ('ep', 'tp'), axis=0, tiled=True)  53.6 us
    reduce_scatter x1, waiting for transfers between devices, per_device_dense(): lax.psum_scatter(head_part, 'tp', scatter_dimension=0, tiled=True)  10.2 us
    pallas_call x1, Pallas kernels, run_experts(): pl.pallas_call(functools.partial(experts_kernel, tp_count, blocks), out_s...  8.19 us
  transfers between devices with their start and end apart: 4, of which 4 were waited for; matrix products, arithmetic and copies ran while one was open for 5% of the time, Pallas kernels for 3%

profile of v1, /device:TPU:0, one launch (start us, length us, event | category | flops | bytes accessed | tf_op | source)
XLA Modules:
  0.0 308.7 jit_solution(7700766673718334661)
XLA Ops:
  7.2 0.0 copy-start
  7.2 0.0 all-gather.3.cloned.1.call-start
  7.2 0.8 constant_dynamic-slice_fusion
  8.1 0.8 constant_dynamic-slice_fusion.1
  8.8 0.1 copy.41
  8.9 0.1 copy.42
  9.0 0.9 fusion.31
  9.9 0.8 constant_dynamic-slice_fusion.2
  10.7 0.1 copy.46
  10.8 0.9 fusion.33
  11.7 0.1 fusion.41
  11.8 0.7 concatenate.13
  12.5 0.0 all-gather.3.cloned.1.call-update
  12.5 0.0 all-gather.5.cloned.1.call-start
  12.6 1.0 fusion.16
  13.6 1.7 fusion.18
  15.3 54.3 %all-gather.3.cloned.1.call-done = bf16[1024,640]{1,0:T(8,128)(2,1)} async-done(((bf16[32,640]{1,0:T(8,128)(2,1)}), bf16[1024,640]{1,0:T(8,128)(2,1)}) %all-gather.3.cloned.1.call-update) | async-done | bytes 1310736 | tf_op jit(solution)/shard_map/all_gather | solution.py:355
  69.7 0.0 copy-start.7
  69.7 0.0 all-gather.5.cloned.1.call-update
  69.7 0.0 reduce-scatter.3.cloned.1.call-start
  69.8 1.1 fusion.13
  70.9 1.6 fusion.22
  72.5 0.1 multiply_cosine_fusion.1
  72.7 0.0 copy-done.7
  72.7 0.0 slice-start
  72.7 1.8 convolution_convert_fusion.1
  74.5 0.0 copy-start.8
  74.6 1.0 copy-done.8
  75.6 0.0 slice-done
  75.6 0.1 copy.44
  75.8 0.0 copy-start.9
  75.8 0.6 multiply_reduce_fusion
  76.3 0.5 fusion
  76.8 0.1 copy-done.9
  77.0 0.6 fusion.3
  77.6 0.0 copy-start.1
  77.6 0.0 copy-start.4
  77.6 0.0 copy-done
  77.6 1.2 convolution_convert_fusion
  78.8 0.0 reduce-scatter.3.cloned.1.call-update
  78.8 0.0 reduce-scatter.5.cloned.1.call-start
  78.9 1.3 convert_add_fusion.scale_ref
  80.2 53.6 %all-gather.5.cloned.1.call-done.rows_ref = bf16[1024,2048]{1,0:T(8,128)(2,1)} async-done(((bf16[32,2048]{1,0:T(8,128)(2,1)}), bf16[1024,2048]{1,0:T(8,128)(2,1)}) %all-gather.5.cloned.1.call-update) | async-done | bytes 4194320 | tf_op jit(solution)/shard_map/all_gather | solution.py:360
  133.8 0.0 copy-done.1
  133.8 0.0 copy-done.4
  133.8 0.0 copy-start.2
  133.8 1.2 copy-done.2
  135.0 0.0 copy-start.3
  135.0 1.2 copy-done.3
  136.2 0.0 copy-start.5
  136.2 1.0 copy-done.5
  137.3 0.0 copy-start.6
  137.3 1.0 copy-done.6
  138.3 8.2 %shard_map.194 = bf16[4096,512]{1,0:T(8,128)(2,1)} custom-call(bf16[1024,2048]{1,0:T(8,128)(2,1)} %all-gather.5.cloned.1.call-done.rows_ref, f32[1024,1]{1,0:T(8,128)S(1)} %convert_add_fusion.scale_ref, bf16[2048,256]{1,0:T(8,128)(2,1)S(1)} %bitcast.17, bf16[2048,256]{1,0:T(8,128)(2,1)S(1)} %bitcast.18, bf16[256,2048]{1,0:T(8,128)(2,1)S(1)} %bitcast.19, ...), custom_call_target="tpu_custom_call" | custom-call | flops 3221225472 | bytes 11534336 | tf_op jit(solution)/shard_map/pallas_call | solution.py:269
  146.5 0.0 copy-start.10
  146.5 0.0 reduce-scatter.5.cloned.1.call-update
  146.5 10.2 %reduce-scatter.3.cloned.1.call-done = bf16[32,2048]{1,0:T(8,128)(2,1)} async-done(((bf16[128,2048]{1,0:T(8,128)(2,1)}), bf16[32,2048]{1,0:T(8,128)(2,1)}) %reduce-scatter.3.cloned.1.call-update) | async-done | bytes 131088 | tf_op jit(solution)/shard_map/reduce_scatter | solution.py:403
  156.7 1.0 fusion.19
  157.8 0.0 copy-done.10
  157.8 1.7 fusion.21
  159.5 142.7 %reduce-scatter.5.cloned.1.call-done = bf16[128,512]{1,0:T(8,128)(2,1)} async-done(((bf16[4096,512]{1,0:T(8,128)(2,1)}), bf16[128,512]{1,0:T(8,128)(2,1)}) %reduce-scatter.5.cloned.1.call-update) | async-done | bytes 131088 | tf_op jit(solution)/shard_map/reduce_scatter | solution.py:424
  (16 shorter events, 0.2 us)
Async XLA Ops:
  7.2 70.5 %copy-start = (bf16[256,2048]{1,0:T(8,128)(2,1)S(1)}, bf16[256,2048]{1,0:T(8,128)(2,1)}, u32[]{:S(2)}) copy-start(bf16[256,2048]{1,0:T(8,128)(2,1)} %param.26) | copy-start | bytes 3145732
  7.2 62.5 %all-gather.3.cloned.1.call-start = ((), (), s32[]{:S(2)}) async-start(), calls=%async_computation.2 | async-start | bytes 1351680 | tf_op jit(solution)/shard_map/all_gather | solution.py:355
  12.5 121.2 %all-gather.5.cloned.1.call-start = ((), (), s32[]{:S(2)}) async-start(), calls=%async_computation.4 | async-start | bytes 4325376 | tf_op jit(solution)/shard_map/all_gather | solution.py:360
  69.7 3.0 copy-start.7
  69.7 87.0 %reduce-scatter.3.cloned.1.call-start = ((), (), s32[]{:S(2)}) async-start(), calls=%async_computation.3 | async-start | bytes 655360 | tf_op jit(solution)/shard_map/reduce_scatter | solution.py:403
  72.7 2.9 slice-start
  74.5 1.0 copy-start.8
  75.8 1.2 copy-start.9
  77.6 56.2 %copy-start.1 = (bf16[1,2048,256]{2,1,0:T(8,128)(2,1)S(1)}, bf16[1,2048,256]{2,1,0:T(8,128)(2,1)}, u32[]{:S(2)}) copy-start(bf16[1,2048,256]{2,1,0:T(8,128)(2,1)} %param.32) | copy-start | bytes 3145732
  77.6 56.2 %copy-start.4 = (bf16[2048,128]{1,0:T(8,128)(2,1)S(1)}, bf16[2048,128]{1,0:T(8,128)(2,1)}, u32[]{:S(2)}) copy-start(bf16[2048,128]{1,0:T(8,128)(2,1)} %shared_gate_ref.1) | copy-start | bytes 1572868
  78.8 223.3 %reduce-scatter.5.cloned.1.call-start = ((), (), s32[]{:S(2)}) async-start(), calls=%async_computation.5 | async-start | bytes 4325376 | tf_op jit(solution)/shard_map/reduce_scatter | solution.py:424
  133.8 1.2 copy-start.2
  135.0 1.2 copy-start.3
  136.2 1.0 copy-start.5
  137.3 1.0 copy-start.6
  146.5 11.3 %copy-start.10 = (f32[2048]{0:T(1024)S(1)}, f32[2048]{0:T(1024)}, u32[]{:S(2)}) copy-start(f32[2048]{0:T(1024)} %param.27) | copy-start | bytes 24580
Sparse Core Ops, SparseCore 0:
  12.7 56.9 all-gather.2
  73.1 60.6 all-gather.4
  136.2 20.4 reduce-scatter.2
  159.4 142.6 reduce-scatter.4

commit v2 on v1

--- a/solution.py
+++ b/solution.py
@@ -204,6 +204,400 @@
     routed = jnp.sum(picked.reshape(tok_rows, top_count, column_part), 1)
     expert_mix = (routed + shared_sum).astype(jnp.bfloat16)
     return (mixed, expert_mix)
+
+
+MESH = pl.DeviceIdType.MESH
+
+
+def grid_of(ep_count, tp_count):
+    y_count = math.gcd(ep_count, 2)
+    k_count = math.gcd(tp_count, 2)
+    return (ep_count // y_count, y_count, tp_count // k_count, k_count)
+
+
+def place_of(dims):
+    ep_at, tp_at = lax.axis_index("ep"), lax.axis_index("tp")
+    return (
+        lax.div(ep_at, dims[1]),
+        lax.rem(ep_at, dims[1]),
+        lax.div(tp_at, dims[3]),
+        lax.rem(tp_at, dims[3]),
+    )
+
+
+def moved(dims, place, dz=0, dy=0, dx=0, dk=0):
+    return tuple(
+        lax.rem(at + step % size, size) if step % size else at
+        for at, step, size in zip(place, (dz, dy, dx, dk), dims)
+    )
+
+
+def device_of(dims, place):
+    return (place[0] * dims[1] + place[1], place[2] * dims[3] + place[3])
+
+
+def block_of(dims, place):
+    ep_at, tp_at = device_of(dims, place)
+    return ep_at * (dims[2] * dims[3]) + tp_at
+
+
+def peers_of(dims):
+    axes = ("dz", "dy", "dx", "dk")
+    return [{axis: step} for axis, size in zip(axes, dims) for step in range(1, size)]
+
+
+def meet(dims, place):
+    barrier = pltpu.get_barrier_semaphore()
+    peers = peers_of(dims)
+    for peer in peers:
+        pl.semaphore_signal(
+            barrier,
+            inc=1,
+            device_id=device_of(dims, moved(dims, place, **peer)),
+            device_id_type=MESH,
+        )
+    pl.semaphore_wait(barrier, len(peers))
+
+
+def far_first(size):
+    return sorted(range(1, size), key=lambda step: -min(step, size - step))
+
+
+def gather_keys(dims):
+    z_count, y_count, x_count, k_count = dims
+    keys = []
+    for dz in range(z_count):
+        keys += [("z", dz, 0, 0, 0)]
+        keys += [("x", dz, 0, dx, 0) for dx in range(1, x_count)]
+        keys += [("y", dz, dy, 0, 0) for dy in range(1, y_count)]
+        for dy in range(y_count):
+            for dx in range(x_count):
+                if dx and dy:
+                    keys += [("p", dz, dy, dx, 0), ("q", dz, dy, dx, 0)]
+                keys += [("k", dz, dy, dx, dk) for dk in range(1, k_count)]
+    return {key: index for index, key in enumerate(keys)}
+
+
+def gather_kernel(dims, *refs):
+    count = (len(refs) - 2) // 2
+    owns, alls, (send_sem, recv_sem) = refs[:count], refs[count : 2 * count], refs[2 * count :]
+    keys = gather_keys(dims)
+    z_count, y_count, x_count, k_count = dims
+    me = place_of(dims)
+    meet(dims, me)
+    sent = []
+
+    def region(which, place, half):
+        rows = owns[which].shape[0]
+        begin = pl.multiple_of(block_of(dims, place) * rows, rows)
+        if half is None:
+            return alls[which].at[pl.ds(begin, rows), :]
+        return alls[which].at[pl.ds(begin + half * (rows // 2), rows // 2), :]
+
+    def describe(which, key, source, place, half, target):
+        return pltpu.make_async_remote_copy(
+            src_ref=source,
+            dst_ref=region(which, place, half),
+            send_sem=send_sem.at[which, keys[key]],
+            recv_sem=recv_sem.at[which, keys[key]],
+            device_id=device_of(dims, target),
+            device_id_type=MESH,
+        )
+
+    def send(which, key, origin, half, **step):
+        source = region(which, origin, half)
+        if origin is me:
+            source = owns[which]
+        copy = describe(which, key, source, origin, half, moved(dims, me, **step))
+        copy.start()
+        sent.append(copy)
+
+    def arrive(which, key, origin, half=None):
+        source = region(which, origin, half)
+        describe(which, key, source, origin, half, me).wait_recv()
+
+    def back(dz=0, dy=0, dx=0, dk=0):
+        if not (dz or dy or dx or dk):
+            return me
+        return moved(dims, me, -dz, -dy, -dx, -dk)
+
+    def to_partner(which, dz, dy, dx):
+        for dk in range(1, k_count):
+            send(which, ("k", dz, dy, dx, dk), back(dz, dy, dx), None, dk=dk)
+
+    order = [0] + far_first(z_count)[::-1]
+    for which in range(count):
+        for dz in far_first(z_count):
+            send(which, ("z", dz, 0, 0, 0), me, None, dz=dz)
+    for which in range(count):
+        for dz in order:
+            if dz:
+                arrive(which, ("z", dz, 0, 0, 0), back(dz))
+            for dx in range(1, x_count):
+                send(which, ("x", dz, 0, dx, 0), back(dz), None, dx=dx)
+            for dy in range(1, y_count):
+                send(which, ("y", dz, dy, 0, 0), back(dz), None, dy=dy)
+            to_partner(which, dz, 0, 0)
+    for which in range(count):
+        alls[which][
+            pl.ds(
+                pl.multiple_of(block_of(dims, me) * owns[which].shape[0], owns[which].shape[0]),
+                owns[which].shape[0],
+            ),
+            :,
+        ] = owns[which][...]
+    for which in range(count):
+        for dz in order:
+            for dx in range(1, x_count):
+                arrive(which, ("x", dz, 0, dx, 0), back(dz, 0, dx))
+                for dy in range(1, y_count):
+                    send(which, ("p", dz, dy, dx, 0), back(dz, 0, dx), 0, dy=dy)
+                to_partner(which, dz, 0, dx)
+            for dy in range(1, y_count):
+                arrive(which, ("y", dz, dy, 0, 0), back(dz, dy, 0))
+                for dx in range(1, x_count):
+                    send(which, ("q", dz, dy, dx, 0), back(dz, dy, 0), 1, dx=dx)
+                to_partner(which, dz, dy, 0)
+    for which in range(count):
+        for dz in order:
+            for dy in range(1, y_count):
+                for dx in range(1, x_count):
+                    arrive(which, ("p", dz, dy, dx, 0), back(dz, dy, dx), 0)
+                    arrive(which, ("q", dz, dy, dx, 0), back(dz, dy, dx), 1)
+                    to_partner(which, dz, dy, dx)
+    for which in range(count):
+        for dz in order:
+            for dy in range(y_count):
+                for dx in range(x_count):
+                    for dk in range(1, k_count):
+                        arrive(which, ("k", dz, dy, dx, dk), back(dz, dy, dx, dk))
+    for copy in sent:
+        copy.wait_send()
+
+
+def gather_all(arrays, ep_count, tp_count):
+    dims = grid_of(ep_count, tp_count)
+    semaphores = (len(arrays), len(gather_keys(dims)))
+    vmem = pl.BlockSpec(memory_space=pltpu.VMEM)
+    return pl.pallas_call(
+        functools.partial(gather_kernel, dims),
+        out_shape=[
+            jax.ShapeDtypeStruct((a.shape[0] * ep_count * tp_count, a.shape[1]), a.dtype)
+            for a in arrays
+        ],
+        in_specs=[vmem] * len(arrays),
+        out_specs=[vmem] * len(arrays),
+        scratch_shapes=[pltpu.SemaphoreType.DMA(semaphores), pltpu.SemaphoreType.DMA(semaphores)],
+        compiler_params=pltpu.CompilerParams(
+            collective_id=0, has_side_effects=True, vmem_limit_bytes=32 * 1024 * 1024
+        ),
+    )(*arrays)
+
+
+def reduce_keys(dims):
+    z_count, y_count, x_count, k_count = dims
+    keys = []
+    for dz in range(z_count):
+        for dy in range(y_count):
+            for dx in range(x_count):
+                keys += [("k", dz, dy, dx, dk) for dk in range(1, k_count)]
+                if dx and dy:
+                    keys += [("p", dz, dy, dx), ("q", dz, dy, dx)]
+                elif dx:
+                    keys += [("x", dz, dx)]
+                elif dy:
+                    keys += [("y", dz, dy)]
+                elif dz:
+                    keys += [("z", dz)]
+    for dx in range(x_count):
+        keys += [("mk", dx, dk) for dk in range(1, k_count)]
+        if dx:
+            keys += [("mx", dx)]
+    return {key: index for index, key in enumerate(keys)}
+
+
+def reduce_slots(dims):
+    slots = {}
+    for key in reduce_keys(dims):
+        group = "pq" if key[0] in "pq" else ("m" if key[0][0] == "m" else "full")
+        taken = sum(1 for other in slots.values() if other[0] == group)
+        slots[key] = (group, taken)
+    sizes = {
+        group: max(1, sum(1 for other in slots.values() if other[0] == group))
+        for group in ("pq", "m", "full")
+    }
+    return slots, sizes
+
+
+def reduce_kernel(
+    dims,
+    parts_ref,
+    head_ref,
+    gain_ref,
+    mixed_ref,
+    out_ref,
+    full,
+    halves,
+    mixes,
+    sums,
+    mix_sums,
+    send_sem,
+    recv_sem,
+):
+    keys = reduce_keys(dims)
+    slots, _ = reduce_slots(dims)
+    stores = {"pq": halves, "m": mixes, "full": full}
+    z_count, y_count, x_count, k_count = dims
+    me = place_of(dims)
+    rows = out_ref.shape[0]
+    half_rows = rows // 2
+    mix_rows = mixed_ref.shape[0]
+    meet(dims, me)
+    sent = []
+
+    def landing(key):
+        group, index = slots[key]
+        return stores[group].at[index]
+
+    def describe(key, source, target):
+        return pltpu.make_async_remote_copy(
+            src_ref=source,
+            dst_ref=landing(key),
+            send_sem=send_sem.at[keys[key]],
+            recv_sem=recv_sem.at[keys[key]],
+            device_id=device_of(dims, target),
+            device_id_type=MESH,
+        )
+
+    def send(key, source, **step):
+        copy = describe(key, source, moved(dims, me, **step))
+        copy.start()
+        sent.append(copy)
+
+    def landed(key):
+        describe(key, landing(key), me).wait_recv()
+        return landing(key)[...].astype(jnp.float32)
+
+    def part_span(dz, dy, dx, dk):
+        begin = block_of(dims, moved(dims, me, dz, dy, dx, dk)) * rows
+        return pl.ds(pl.multiple_of(begin, rows), rows)
+
+    def mix_span(dx, dk):
+        begin = device_of(dims, moved(dims, me, dx=dx, dk=dk))[1] * mix_rows
+        return pl.ds(pl.multiple_of(begin, mix_rows), mix_rows)
+
+    z_order = far_first(z_count) + [0]
+    z_steps = z_order
+    diagonal = [
+        (dz, dy, dx) for dz in z_steps for dy in range(1, y_count) for dx in range(1, x_count)
+    ]
+    side_x = [(dz, 0, dx) for dz in z_steps for dx in range(1, x_count)]
+    side_y = [(dz, dy, 0) for dz in z_steps for dy in range(1, y_count)]
+    straight = [(dz, 0, 0) for dz in z_steps]
+
+    for place in diagonal[:1]:
+        for dk in range(1, k_count):
+            send(("k", *place, dk), parts_ref.at[part_span(*place, dk)], dk=dk)
+    for dx in range(x_count):
+        for dk in range(1, k_count):
+            send(("mk", dx, dk), head_ref.at[mix_span(dx, dk)], dk=dk)
+    for place in diagonal[1:] + side_x + side_y + straight:
+        for dk in range(1, k_count):
+            send(("k", *place, dk), parts_ref.at[part_span(*place, dk)], dk=dk)
+
+    def core_sum(place):
+        value = parts_ref[part_span(*place, 0), :].astype(jnp.float32)
+        for dk in range(1, k_count):
+            value = value + landed(("k", *place, dk))
+        return value
+
+    index_of = {}
+
+    def keep(place, value):
+        index_of[place] = len(index_of)
+        sums[index_of[place]] = value.astype(jnp.bfloat16)
+        return index_of[place]
+
+    def mix_core(dx):
+        value = head_ref[mix_span(dx, 0), :].astype(jnp.float32)
+        for dk in range(1, k_count):
+            value = value + landed(("mk", dx, dk))
+        return value
+
+    for dx in range(1, x_count):
+        mix_sums[dx - 1] = mix_core(dx).astype(jnp.bfloat16)
+        send(("mx", dx), mix_sums.at[dx - 1], dx=dx)
+    for place in diagonal:
+        dz, dy, dx = place
+        index = keep(place, core_sum(place))
+        send(("p", dz, dy, dx), sums.at[index, pl.ds(0, half_rows)], dy=dy)
+        send(("q", dz, dy, dx), sums.at[index, pl.ds(half_rows, half_rows)], dx=dx)
+    for dz in z_steps:
+        for dx in range(1, x_count):
+            value = core_sum((dz, 0, dx))
+            upper, lower = value[:half_rows], value[half_rows:]
+            for dy in range(1, y_count):
+                upper = upper + landed(("p", dz, dy, dx))
+            index = keep((dz, 0, dx), jnp.concatenate([upper, lower], 0))
+            send(("x", dz, dx), sums.at[index], dx=dx)
+        for dy in range(1, y_count):
+            value = core_sum((dz, dy, 0))
+            upper, lower = value[:half_rows], value[half_rows:]
+            for dx in range(1, x_count):
+                lower = lower + landed(("q", dz, dy, dx))
+            index = keep((dz, dy, 0), jnp.concatenate([upper, lower], 0))
+            send(("y", dz, dy), sums.at[index], dy=dy)
+    mixture = mix_core(0)
+    for dx in range(1, x_count):
+        mixture = mixture + landed(("mx", dx))
+    scale = lax.rsqrt(jnp.mean(mixture * mixture, -1, keepdims=True) + EPS)
+    mixed_ref[...] = (mixture * scale * gain_ref[...]).astype(jnp.bfloat16)
+    for dz in z_steps:
+        value = core_sum((dz, 0, 0))
+        for dx in range(1, x_count):
+            value = value + landed(("x", dz, dx))
+        for dy in range(1, y_count):
+            value = value + landed(("y", dz, dy))
+        if dz:
+            index = keep((dz, 0, 0), value)
+            send(("z", dz), sums.at[index], dz=dz)
+    for dz in range(1, z_count):
+        value = value + landed(("z", dz))
+    out_ref[...] = value.astype(jnp.bfloat16)
+    for copy in sent:
+        copy.wait_send()
+
+
+def reduce_all(parts, head_part, gain, ep_count, tp_count):
+    dims = grid_of(ep_count, tp_count)
+    _, sizes = reduce_slots(dims)
+    rows = parts.shape[0] // (ep_count * tp_count)
+    width = parts.shape[1]
+    mix_rows = head_part.shape[0] // tp_count
+    mix_width = head_part.shape[1]
+    vmem = pl.BlockSpec(memory_space=pltpu.VMEM)
+    semaphores = pltpu.SemaphoreType.DMA((len(reduce_keys(dims)),))
+    return pl.pallas_call(
+        functools.partial(reduce_kernel, dims),
+        out_shape=[
+            jax.ShapeDtypeStruct((mix_rows, mix_width), jnp.bfloat16),
+            jax.ShapeDtypeStruct((rows, width), jnp.bfloat16),
+        ],
+        in_specs=[vmem] * 3,
+        out_specs=[vmem] * 2,
+        scratch_shapes=[
+            pltpu.VMEM((sizes["full"], rows, width), jnp.bfloat16),
+            pltpu.VMEM((sizes["pq"], rows // 2, width), jnp.bfloat16),
+            pltpu.VMEM((sizes["m"], mix_rows, mix_width), jnp.bfloat16),
+            pltpu.VMEM((dims[0] * dims[1] * dims[2], rows, width), jnp.bfloat16),
+            pltpu.VMEM((max(1, dims[2] - 1), mix_rows, mix_width), jnp.bfloat16),
+            semaphores,
+            semaphores,
+        ],
+        compiler_params=pltpu.CompilerParams(
+            collective_id=1, has_side_effects=True, vmem_limit_bytes=48 * 1024 * 1024
+        ),
+    )(parts, head_part, gain)
 
 
 def experts_kernel(
@@ -352,12 +746,10 @@
     packed = jnp.concatenate(
         [own_latent, own_rot, dense_high, dense_low, jnp.zeros((quarter, fill), jnp.bfloat16)], 1
     )
-    packed = lax.all_gather(packed, ("ep", "tp"), axis=0, tiled=True)
     own_normed = rms_scale(
         lax.dynamic_slice_in_dim(second_rows, second_offset, second_quarter, 0), second_gain
     )
-    own_normed, packed = lax.optimization_barrier((own_normed, packed))
-    normed = lax.all_gather(own_normed, ("ep", "tp"), axis=0, tiled=True)
+    packed, normed = gather_all([packed, own_normed], ep_count, tp_count)
 
     positions = start_row.astype(jnp.float32) + jnp.arange(first_rows, dtype=jnp.float32)
     queries = jnp.dot(
@@ -400,10 +792,6 @@
     head_part = jnp.dot(attended, output_weight, preferred_element_type=jnp.float32).astype(
         jnp.bfloat16
     )
-    mixture = lax.psum_scatter(head_part, "tp", scatter_dimension=0, tiled=True).astype(
-        jnp.float32
-    )
-    mixed = rms_scale(mixture, output_gain)
 
     me = lax.axis_index("ep")
     high = lax.dynamic_slice_in_dim(packed, latent_width + ROPE + me, 1, 1)
@@ -421,7 +809,9 @@
         ep_count,
         tp_count,
     )
-    expert_mix = lax.psum_scatter(parts, ("ep", "tp"), scatter_dimension=0, tiled=True)
+    mixed, expert_mix = reduce_all(
+        parts, head_part, output_gain.reshape(1, -1), ep_count, tp_count
+    )
     return (mixed, expert_mix)
 
 

time: 309 us -> 105 us (0.34)
  waiting for transfers between devices: 261 us -> 0 us
  Pallas kernels: 8.19 us -> 78.9 us
  between operations: 14 us -> 0.89 us
  local copies, waits for them, and re-layouts: 9.24 us -> 14 us
  other arithmetic: 10.4 us -> 6.14 us
    reduce_scatter x2 -> x0, waiting for transfers between devices: 153 us -> none  [the longest x1 143 us: per_device_dense(): lax.psum_scatter(parts, ('ep', 'tp'), scatter_dimension=0, tiled=True)]
    all_gather x2 -> x0, waiting for transfers between devices: 108 us -> none  [the longest x1 54.3 us: per_device_dense(): packed = lax.all_gather(packed, ('ep', 'tp'), axis=0, tiled=True)]
    pallas_call x0 -> x2, Pallas kernels: none -> 70.8 us  [the longest x1 35.6 us: reduce_all(): pl.pallas_call(functools.partial(reduce_kernel, dims), out_shape=[jax.Sha...]
    unnamed x23 -> x35, local copies, waits for them, and re-layouts: 5.8 us -> 11.2 us
  transfers between devices with their start and end apart: 4 -> 0, of which waited for: 4 -> 0; matrix products, arithmetic and copies ran while one was open for 5% -> 0% of each run, Pallas kernels for 3% -> 0%
where the time goes in v2:
time: 105 us; the launch traced here: 104 us
  Pallas kernels  78.9 us (75%)
  local copies, waits for them, and re-layouts  14 us (13%)
  other arithmetic  6.14 us (6%)
  matrix products  4.16 us (4%)
    pallas_call x1, Pallas kernels, reduce_all(): pl.pallas_call(functools.partial(reduce_kernel, dims), out_shape=[jax.Sha...  35.6 us
    pallas_call x1, Pallas kernels, gather_all(): pl.pallas_call(functools.partial(gather_kernel, dims), out_shape=[jax.Sha...  35.1 us
    unnamed x35, local copies, waits for them, and re-layouts  11.2 us
    pallas_call x1, Pallas kernels, run_experts(): pl.pallas_call(functools.partial(experts_kernel, tp_count, blocks), out_s...  8.19 us
    dot_general x1, matrix products, per_device_dense(): jnp.dot(all_latent, keyval_weight, preferred_element_type=jnp.float32)  2.27 us

profile of v2, /device:TPU:0, one launch (start us, length us, event | category | flops | bytes accessed | tf_op | source)
XLA Modules:
  0.0 104.2 jit_solution(15673198929604093403)
XLA Ops:
  0.6 0.0 copy-start
  0.7 0.8 constant_dynamic-slice_fusion
  1.5 0.8 constant_dynamic-slice_fusion.1
  2.3 0.1 copy.42
  2.4 0.1 copy.41
  2.4 0.9 fusion.28
  3.3 0.9 fusion.30
  4.2 0.8 constant_dynamic-slice_fusion.2
  5.0 0.1 copy.46
  5.1 0.1 fusion.38
  5.2 0.1 concatenate.13.refs_0_
  5.3 1.0 fusion.16
  6.4 1.0 fusion.18.refs_1_
  7.4 35.1 %shard_map.194 = (bf16[1024,640]{1,0:T(8,128)(2,1)S(1)}, bf16[1024,2048]{1,0:T(8,128)(2,1)S(1)}) custom-call(bf16[32,640]{1,0:T(8,128)(2,1)S(1)} %concatenate.13.refs_0_, bf16[32,2048]{1,0:T(8,128)(2,1)S(1)} %fusion.18.refs_1_), custom_call_target="tpu_custom_call" | custom-call | tf_op jit(solution)/shard_map/pallas_call | solution.py:382
  42.6 0.0 copy-start.2
  42.6 1.9 %copy-done.2 = bf16[1024,2048]{1,0:T(8,128)(2,1)} copy-done((bf16[1024,2048]{1,0:T(8,128)(2,1)}, bf16[1024,2048]{1,0:T(8,128)(2,1)S(1)}, u32[]{:S(2)}) %copy-start.2) | copy-done | bytes 4194328
  44.5 0.0 copy-start.9
  44.5 0.0 copy-start.11
  44.5 0.0 copy-start.12
  44.5 0.0 copy-start.15
  44.5 2.3 %convolution_convert_fusion.1 = bf16[1024,512]{0,1:T(8,128)(2,1)S(1)} fusion(bf16[512,512]{1,0:T(8,128)(2,1)} %param.25, bf16[1024,640]{1,0:T(8,128)(2,1)S(1)} %get-tuple-element.5), kind=kOutput, calls=%fused_computation.5 | convolution fusion | flops 537395200 | bytes 2621440 | tf_op jit(solution)/shard_map/dot_general | solution.py:765
  46.8 0.0 copy-start.13
  46.8 0.0 copy-done.9
  46.9 0.9 copy-done.13
  47.8 0.1 copy.44
  48.0 0.1 multiply_cosine_fusion.1
  48.1 0.0 copy-done.11
  48.1 0.1 fusion.13
  48.3 0.0 copy-done.12
  48.3 0.0 copy-done.15
  48.3 0.4 fusion.19
  48.7 0.0 copy-start.14
  48.7 0.6 multiply_reduce_fusion
  49.3 0.5 fusion
  49.8 0.1 copy-done.14
  50.0 0.6 fusion.3
  50.6 0.0 copy-start.3
  50.6 0.0 copy-start.6
  50.6 0.0 copy-done
  50.6 0.3 convolution_convert_fusion.head_ref
  50.9 1.3 %convert_add_fusion.scale_ref = f32[1024,1]{1,0:T(8,128)S(1)} fusion(bf16[1024,640]{1,0:T(8,128)(2,1)} %copy-done.9, s32[]{:T(128)S(6)} %select_n.20, s32[]{:T(128)S(6)} %select_n.19), kind=kLoop, calls=%fused_computation.17 | loop fusion | flops 3072 | bytes 8200 | tf_op jit(solution)/shard_map/add | solution.py:799
  52.3 0.0 copy-done.3
  52.3 0.0 copy-done.6
  52.3 0.0 copy-start.4
  52.3 1.2 %copy-done.4 = bf16[1,2048,256]{2,1,0:T(8,128)(2,1)S(1)} copy-done((bf16[1,2048,256]{2,1,0:T(8,128)(2,1)S(1)}, bf16[1,2048,256]{2,1,0:T(8,128)(2,1)}, u32[]{:S(2)}) %copy-start.4) | copy-done | bytes 1048600
  53.5 0.0 copy-start.5
  53.5 1.2 %copy-done.5 = bf16[1,256,2048]{2,1,0:T(8,128)(2,1)S(1)} copy-done((bf16[1,256,2048]{2,1,0:T(8,128)(2,1)S(1)}, bf16[1,256,2048]{2,1,0:T(8,128)(2,1)}, u32[]{:S(2)}) %copy-start.5) | copy-done | bytes 1048600
  54.7 0.0 copy-start.7
  54.7 1.0 copy-done.7
  55.8 0.0 copy-start.8
  55.8 1.0 copy-done.8
  56.8 0.0 copy-start.10
  56.8 8.2 %shard_map.195.parts_ref = bf16[4096,512]{1,0:T(8,128)(2,1)} custom-call(bf16[1024,2048]{1,0:T(8,128)(2,1)} %copy-done.2, f32[1024,1]{1,0:T(8,128)S(1)} %convert_add_fusion.scale_ref, bf16[2048,256]{1,0:T(8,128)(2,1)S(1)} %bitcast.18, bf16[2048,256]{1,0:T(8,128)(2,1)S(1)} %bitcast.19, bf16[256,2048]{1,0:T(8,128)(2,1)S(1)} %bitcast.20, ...), custom_call_target="tpu_custom_call" | custom-call | flops 3221225472 | bytes 11534336 | tf_op jit(solution)/shard_map/pallas_call | solution.py:663
  65.0 0.0 copy-done.10
  65.0 0.0 copy-start.1
  65.0 2.2 %copy-done.1 = bf16[4096,512]{1,0:T(8,128)(2,1)S(1)} copy-done((bf16[4096,512]{1,0:T(8,128)(2,1)S(1)}, bf16[4096,512]{1,0:T(8,128)(2,1)}, u32[]{:S(2)}) %copy-start.1) | copy-done | bytes 4194328
  67.2 35.6 %shard_map.196 = (bf16[32,2048]{1,0:T(8,128)(2,1)S(1)}, bf16[128,512]{1,0:T(8,128)(2,1)S(1)}) custom-call(bf16[4096,512]{1,0:T(8,128)(2,1)S(1)} %copy-done.1, bf16[128,2048]{1,0:T(8,128)(2,1)S(1)} %convolution_convert_fusion.head_ref, f32[1,2048]{1,0:T(1,128)S(1)} %bitcast.21), custom_call_target="tpu_custom_call" | custom-call | tf_op jit(solution)/shard_map/pallas_call | solution.py:580
  102.8 0.7 copy.49
  103.5 0.7 copy.50
  (16 shorter events, 0.2 us)
Async XLA Ops:
  0.6 49.9 %copy-start = (bf16[256,2048]{1,0:T(8,128)(2,1)S(1)}, bf16[256,2048]{1,0:T(8,128)(2,1)}, u32[]{:S(2)}) copy-start(bf16[256,2048]{1,0:T(8,128)(2,1)} %param.26) | copy-start | bytes 3145732
  42.6 1.9 %copy-start.2 = (bf16[1024,2048]{1,0:T(8,128)(2,1)}, bf16[1024,2048]{1,0:T(8,128)(2,1)S(1)}, u32[]{:S(2)}) copy-start(bf16[1024,2048]{1,0:T(8,128)(2,1)S(1)} %get-tuple-element.4.rows_ref) | copy-start | bytes 12582916
  44.5 2.3 %copy-start.9 = (bf16[1024,640]{1,0:T(8,128)(2,1)}, bf16[1024,640]{1,0:T(8,128)(2,1)S(1)}, u32[]{:S(2)}) copy-start(bf16[1024,640]{1,0:T(8,128)(2,1)S(1)} %get-tuple-element.5) | copy-start | bytes 3932164
  44.5 3.6 %copy-start.11 = (bf16[128,768]{1,0:T(8,128)(2,1)S(1)}, bf16[128,768]{1,0:T(8,128)(2,1)}, u32[]{:S(2)}) copy-start(bf16[128,768]{1,0:T(8,128)(2,1)} %param.19) | copy-start | bytes 589828
  44.5 3.7 %copy-start.12 = (bf16[768,384]{1,0:T(8,128)(2,1)S(1)}, bf16[768,384]{1,0:T(8,128)(2,1)}, u32[]{:S(2)}) copy-start(bf16[768,384]{1,0:T(8,128)(2,1)} %param.24) | copy-start | bytes 1769476
  44.5 3.7 %copy-start.15 = (f32[768]{0:T(1024)S(1)}, f32[768]{0:T(1024)}, u32[]{:S(2)}) copy-start(f32[768]{0:T(1024)} %param.22) | copy-start | bytes 9220
  46.8 1.0 copy-start.13
  48.7 1.2 %copy-start.14 = (bf16[1024,512]{0,1:T(8,128)(2,1)S(1)}, bf16[1024,512]{0,1:T(8,128)(2,1)}, u32[]{:S(2)}) copy-start(bf16[1024,512]{0,1:T(8,128)(2,1)} %copy-done.13) | copy-start | bytes 3145732
  50.6 1.7 %copy-start.3 = (bf16[1,2048,256]{2,1,0:T(8,128)(2,1)S(1)}, bf16[1,2048,256]{2,1,0:T(8,128)(2,1)}, u32[]{:S(2)}) copy-start(bf16[1,2048,256]{2,1,0:T(8,128)(2,1)} %param.32) | copy-start | bytes 3145732
  50.6 1.7 %copy-start.6 = (bf16[2048,128]{1,0:T(8,128)(2,1)S(1)}, bf16[2048,128]{1,0:T(8,128)(2,1)}, u32[]{:S(2)}) copy-start(bf16[2048,128]{1,0:T(8,128)(2,1)} %shared_gate_ref.1) | copy-start | bytes 1572868
  52.3 1.2 %copy-start.4 = (bf16[1,2048,256]{2,1,0:T(8,128)(2,1)S(1)}, bf16[1,2048,256]{2,1,0:T(8,128)(2,1)}, u32[]{:S(2)}) copy-start(bf16[1,2048,256]{2,1,0:T(8,128)(2,1)} %param.33) | copy-start | bytes 3145732
  53.5 1.2 %copy-start.5 = (bf16[1,256,2048]{2,1,0:T(8,128)(2,1)S(1)}, bf16[1,256,2048]{2,1,0:T(8,128)(2,1)}, u32[]{:S(2)}) copy-start(bf16[1,256,2048]{2,1,0:T(8,128)(2,1)} %param.34) | copy-start | bytes 3145732
  54.7 1.0 %copy-start.7 = (bf16[2048,128]{1,0:T(8,128)(2,1)S(1)}, bf16[2048,128]{1,0:T(8,128)(2,1)}, u32[]{:S(2)}) copy-start(bf16[2048,128]{1,0:T(8,128)(2,1)} %shared_up_ref.1) | copy-start | bytes 1572868
  55.8 1.0 %copy-start.8 = (bf16[128,2048]{1,0:T(8,128)(2,1)S(1)}, bf16[128,2048]{1,0:T(8,128)(2,1)}, u32[]{:S(2)}) copy-start(bf16[128,2048]{1,0:T(8,128)(2,1)} %shared_down_ref.1) | copy-start | bytes 1572868
  56.8 8.2 %copy-start.10 = (f32[2048]{0:T(1024)S(1)}, f32[2048]{0:T(1024)}, u32[]{:S(2)}) copy-start(f32[2048]{0:T(1024)} %param.27) | copy-start | bytes 24580
  65.0 2.2 %copy-start.1 = (bf16[4096,512]{1,0:T(8,128)(2,1)S(1)}, bf16[4096,512]{1,0:T(8,128)(2,1)}, u32[]{:S(2)}) copy-start(bf16[4096,512]{1,0:T(8,128)(2,1)} %shard_map.195.parts_ref) | copy-start | bytes 12582916

commit v3 on v2

--- a/solution.py
+++ b/solution.py
@@ -431,11 +431,19 @@
 
 def reduce_kernel(
     dims,
-    parts_ref,
+    rows_ref,
+    scale_ref,
+    gate_ref,
+    up_ref,
+    down_ref,
+    shared_gate_ref,
+    shared_up_ref,
+    shared_down_ref,
     head_ref,
     gain_ref,
     mixed_ref,
     out_ref,
+    parts_ref,
     full,
     halves,
     mixes,
@@ -478,35 +486,48 @@
         describe(key, landing(key), me).wait_recv()
         return landing(key)[...].astype(jnp.float32)
 
-    def part_span(dz, dy, dx, dk):
-        begin = block_of(dims, moved(dims, me, dz, dy, dx, dk)) * rows
-        return pl.ds(pl.multiple_of(begin, rows), rows)
+    def part_of(dz, dy, dx, dk):
+        column = device_of(dims, moved(dims, me, dx=dx, dk=dk))[1]
+        return parts_ref.at[dz * y_count + dy, column]
+
+    def compute(dz, dy):
+        begin = device_of(dims, moved(dims, me, dz=dz, dy=dy))[0] * rows
+        span = pl.ds(pl.multiple_of(begin, rows), rows)
+        tokens = rows_ref[span, :]
+        gate_act = jnp.dot(tokens, gate_ref[...], preferred_element_type=jnp.float32)
+        up_act = jnp.dot(tokens, up_ref[...], preferred_element_type=jnp.float32)
+        hidden = gate_act / (1.0 + jnp.exp(-gate_act)) * up_act * scale_ref[span, :]
+        hidden = hidden.astype(jnp.bfloat16)
+        own = dz == 0 and dy == 0
+        if own:
+            gate_own = jnp.dot(tokens, shared_gate_ref[...], preferred_element_type=jnp.float32)
+            up_own = jnp.dot(tokens, shared_up_ref[...], preferred_element_type=jnp.float32)
+            hidden_own = gate_own / (1.0 + jnp.exp(-gate_own)) * up_own
+            hidden_own = hidden_own.astype(jnp.bfloat16)
+        part = out_ref.shape[1]
+        for column in range(x_count * k_count):
+            columns = pl.ds(column * part, part)
+            value = jnp.dot(hidden, down_ref[:, columns], preferred_element_type=jnp.float32)
+            if own:
+                value += jnp.dot(
+                    hidden_own, shared_down_ref[:, columns], preferred_element_type=jnp.float32
+                )
+            parts_ref[dz * y_count + dy, column] = value.astype(jnp.bfloat16)
+        for dx in range(x_count - 1, -1, -1):
+            for dk in range(1, k_count):
+                send(("k", dz, dy, dx, dk), part_of(dz, dy, dx, dk), dk=dk)
 
     def mix_span(dx, dk):
         begin = device_of(dims, moved(dims, me, dx=dx, dk=dk))[1] * mix_rows
         return pl.ds(pl.multiple_of(begin, mix_rows), mix_rows)
 
-    z_order = far_first(z_count) + [0]
-    z_steps = z_order
-    diagonal = [
-        (dz, dy, dx) for dz in z_steps for dy in range(1, y_count) for dx in range(1, x_count)
-    ]
-    side_x = [(dz, 0, dx) for dz in z_steps for dx in range(1, x_count)]
-    side_y = [(dz, dy, 0) for dz in z_steps for dy in range(1, y_count)]
-    straight = [(dz, 0, 0) for dz in z_steps]
-
-    for place in diagonal[:1]:
-        for dk in range(1, k_count):
-            send(("k", *place, dk), parts_ref.at[part_span(*place, dk)], dk=dk)
+    z_steps = far_first(z_count) + [0]
     for dx in range(x_count):
         for dk in range(1, k_count):
             send(("mk", dx, dk), head_ref.at[mix_span(dx, dk)], dk=dk)
-    for place in diagonal[1:] + side_x + side_y + straight:
-        for dk in range(1, k_count):
-            send(("k", *place, dk), parts_ref.at[part_span(*place, dk)], dk=dk)
 
     def core_sum(place):
-        value = parts_ref[part_span(*place, 0), :].astype(jnp.float32)
+        value = part_of(*place, 0)[...].astype(jnp.float32)
         for dk in range(1, k_count):
             value = value + landed(("k", *place, dk))
         return value
@@ -524,29 +545,38 @@
             value = value + landed(("mk", dx, dk))
         return value
 
-    for dx in range(1, x_count):
-        mix_sums[dx - 1] = mix_core(dx).astype(jnp.bfloat16)
-        send(("mx", dx), mix_sums.at[dx - 1], dx=dx)
-    for place in diagonal:
-        dz, dy, dx = place
-        index = keep(place, core_sum(place))
-        send(("p", dz, dy, dx), sums.at[index, pl.ds(0, half_rows)], dy=dy)
-        send(("q", dz, dy, dx), sums.at[index, pl.ds(half_rows, half_rows)], dx=dx)
-    for dz in z_steps:
+    def finish(dz, dy):
+        if dy:
+            for dx in range(1, x_count):
+                index = keep((dz, dy, dx), core_sum((dz, dy, dx)))
+                send(("p", dz, dy, dx), sums.at[index, pl.ds(0, half_rows)], dy=dy)
+                send(("q", dz, dy, dx), sums.at[index, pl.ds(half_rows, half_rows)], dx=dx)
+            return
+        for over in range(1, y_count):
+            value = core_sum((dz, over, 0))
+            upper, lower = value[:half_rows], value[half_rows:]
+            for dx in range(1, x_count):
+                lower = lower + landed(("q", dz, over, dx))
+            index = keep((dz, over, 0), jnp.concatenate([upper, lower], 0))
+            send(("y", dz, over), sums.at[index], dy=over)
         for dx in range(1, x_count):
             value = core_sum((dz, 0, dx))
             upper, lower = value[:half_rows], value[half_rows:]
-            for dy in range(1, y_count):
-                upper = upper + landed(("p", dz, dy, dx))
+            for over in range(1, y_count):
+                upper = upper + landed(("p", dz, over, dx))
             index = keep((dz, 0, dx), jnp.concatenate([upper, lower], 0))
             send(("x", dz, dx), sums.at[index], dx=dx)
-        for dy in range(1, y_count):
-            value = core_sum((dz, dy, 0))
-            upper, lower = value[:half_rows], value[half_rows:]
+
+    blocks = [(dz, dy) for dy in list(range(1, y_count)) + [0] for dz in z_steps]
+    for turn, block in enumerate(blocks):
+        compute(*block)
+        if turn:
+            finish(*blocks[turn - 1])
+        else:
             for dx in range(1, x_count):
-                lower = lower + landed(("q", dz, dy, dx))
-            index = keep((dz, dy, 0), jnp.concatenate([upper, lower], 0))
-            send(("y", dz, dy), sums.at[index], dy=dy)
+                mix_sums[dx - 1] = mix_core(dx).astype(jnp.bfloat16)
+                send(("mx", dx), mix_sums.at[dx - 1], dx=dx)
+    finish(*blocks[-1])
     mixture = mix_core(0)
     for dx in range(1, x_count):
         mixture = mixture + landed(("mx", dx))
@@ -568,11 +598,12 @@
         copy.wait_send()
 
 
-def reduce_all(parts, head_part, gain, ep_count, tp_count):
+def reduce_all(expert_args, head_part, gain, ep_count, tp_count):
     dims = grid_of(ep_count, tp_count)
     _, sizes = reduce_slots(dims)
-    rows = parts.shape[0] // (ep_count * tp_count)
-    width = parts.shape[1]
+    count, model_width = expert_args[0].shape
+    rows = count // ep_count
+    width = model_width // tp_count
     mix_rows = head_part.shape[0] // tp_count
     mix_width = head_part.shape[1]
     vmem = pl.BlockSpec(memory_space=pltpu.VMEM)
@@ -583,9 +614,10 @@
             jax.ShapeDtypeStruct((mix_rows, mix_width), jnp.bfloat16),
             jax.ShapeDtypeStruct((rows, width), jnp.bfloat16),
         ],
-        in_specs=[vmem] * 3,
+        in_specs=[vmem] * (len(expert_args) + 2),
         out_specs=[vmem] * 2,
         scratch_shapes=[
+            pltpu.VMEM((ep_count, tp_count, rows, width), jnp.bfloat16),
             pltpu.VMEM((sizes["full"], rows, width), jnp.bfloat16),
             pltpu.VMEM((sizes["pq"], rows // 2, width), jnp.bfloat16),
             pltpu.VMEM((sizes["m"], mix_rows, mix_width), jnp.bfloat16),
@@ -597,94 +629,7 @@
         compiler_params=pltpu.CompilerParams(
             collective_id=1, has_side_effects=True, vmem_limit_bytes=48 * 1024 * 1024
         ),
-    )(parts, head_part, gain)
-
-
-def experts_kernel(
-    tp_count,
-    blocks,
-    rows_ref,
-    scale_ref,
-    gate_ref,
-    up_ref,
-    down_ref,
-    shared_gate_ref,
-    shared_up_ref,
-    shared_down_ref,
-    out_ref,
-    total,
-):
-    step = pl.program_id(0)
-    me = lax.axis_index("ep")
-    tile = rows_ref.shape[0]
-    block_rows = tile // blocks
-    width = down_ref.shape[1]
-    part = width // tp_count
-    rows = rows_ref[...]
-    gate_act = jnp.dot(rows, gate_ref[...], preferred_element_type=jnp.float32)
-    up_act = jnp.dot(rows, up_ref[...], preferred_element_type=jnp.float32)
-    hidden = gate_act / (1.0 + jnp.exp(-gate_act)) * up_act * scale_ref[...]
-    total[...] = jnp.dot(
-        hidden.astype(jnp.bfloat16), down_ref[...], preferred_element_type=jnp.float32
-    )
-
-    for block in range(blocks):
-
-        @pl.when(step * blocks + block == me)
-        def _():
-            span = pl.ds(block * block_rows, block_rows)
-            own = rows_ref[span, :]
-            gate_own = jnp.dot(own, shared_gate_ref[...], preferred_element_type=jnp.float32)
-            up_own = jnp.dot(own, shared_up_ref[...], preferred_element_type=jnp.float32)
-            hidden_own = gate_own / (1.0 + jnp.exp(-gate_own)) * up_own
-            total[span, :] += jnp.dot(
-                hidden_own.astype(jnp.bfloat16),
-                shared_down_ref[...],
-                preferred_element_type=jnp.float32,
-            )
-
-    for block in range(blocks):
-        for column in range(tp_count):
-            out_ref[pl.ds((block * tp_count + column) * block_rows, block_rows), :] = total[
-                block * block_rows : (block + 1) * block_rows, column * part : (column + 1) * part
-            ].astype(jnp.bfloat16)
-
-
-def run_experts(rows, scale, gate, up, down, shared_gate, shared_up, shared_down, ep_count, tp_count):
-    count, width = rows.shape
-    block_rows = count // ep_count
-    blocks = math.gcd(ep_count, 2)
-    tile = block_rows * blocks
-    part = width // tp_count
-
-    def whole(array):
-        return pl.BlockSpec(array.shape, lambda i: (0, 0))
-
-    return pl.pallas_call(
-        functools.partial(experts_kernel, tp_count, blocks),
-        out_shape=jax.ShapeDtypeStruct((count * tp_count, part), jnp.bfloat16),
-        grid=(count // tile,),
-        in_specs=[
-            pl.BlockSpec((tile, width), lambda i: (i, 0)),
-            pl.BlockSpec((tile, 1), lambda i: (i, 0)),
-            whole(gate),
-            whole(up),
-            whole(down),
-            whole(shared_gate),
-            whole(shared_up),
-            whole(shared_down),
-        ],
-        out_specs=pl.BlockSpec((tile * tp_count, part), lambda i: (i, 0)),
-        scratch_shapes=[pltpu.VMEM((tile, width), jnp.float32)],
-        compiler_params=pltpu.CompilerParams(
-            dimension_semantics=("arbitrary",), vmem_limit_bytes=48 * 1024 * 1024
-        ),
-        cost_estimate=pl.CostEstimate(
-            flops=6 * count * width * gate.shape[1],
-            bytes_accessed=4 * count * width + 6 * width * gate.shape[1],
-            transcendentals=count * gate.shape[1],
-        ),
-    )(rows, scale, gate, up, down, shared_gate, shared_up, shared_down)
+    )(*expert_args, head_part, gain)
 
 
 def per_device_dense(
@@ -797,7 +742,7 @@
     high = lax.dynamic_slice_in_dim(packed, latent_width + ROPE + me, 1, 1)
     low = lax.dynamic_slice_in_dim(packed, latent_width + ROPE + ep_count + me, 1, 1)
     scale = high.astype(jnp.float32) + low.astype(jnp.float32)
-    parts = run_experts(
+    expert_args = (
         normed,
         scale,
         gate_weight[0],
@@ -806,11 +751,9 @@
         shared_gate,
         shared_up,
         shared_down,
-        ep_count,
-        tp_count,
     )
     mixed, expert_mix = reduce_all(
-        parts, head_part, output_gain.reshape(1, -1), ep_count, tp_count
+        expert_args, head_part, output_gain.reshape(1, -1), ep_count, tp_count
     )
     return (mixed, expert_mix)
 

time: 105 us -> 91.3 us (0.87)
  local copies, waits for them, and re-layouts: 14 us -> 7.28 us
  Pallas kernels: 78.9 us -> 72.9 us
    pallas_call x1 -> x0, Pallas kernels: 8.19 us -> none  [run_experts(): pl.pallas_call(functools.partial(experts_kernel, tp_count, blocks), out_s...]
    unnamed x35 -> x23, local copies, waits for them, and re-layouts: 11.2 us -> 4.52 us
    pallas_call x1, Pallas kernels: 35.6 us -> 37.7 us  [reduce_all(): pl.pallas_call(functools.partial(reduce_kernel, dims), out_shape=[jax.Sha...]
    dot_general x1, matrix products: 2.27 us -> 0.75 us  [per_device_dense(): jnp.dot(all_latent, keyval_weight, preferred_element_type=jnp.float32)]
    dot_general x1, matrix products: 0.41 us -> 1.6 us  [per_device_dense(): jnp.dot(rms_scale(query_latent, query_gain), query_weight, preferred_elem...]
    add x1, other arithmetic: 1.34 us -> 0.21 us  [per_device_dense(): scale = high.astype(jnp.float32) + low.astype(jnp.float32)]
where the time goes in v3:
time: 91.3 us; the launch traced here: 90.9 us
  Pallas kernels  72.9 us (80%)
  local copies, waits for them, and re-layouts  7.28 us (8%)
  other arithmetic  6.01 us (7%)
  matrix products  3.84 us (4%)
    pallas_call x1, Pallas kernels, reduce_all(): pl.pallas_call(functools.partial(reduce_kernel, dims), out_shape=[jax.Sha...  37.7 us
    pallas_call x1, Pallas kernels, gather_all(): pl.pallas_call(functools.partial(gather_kernel, dims), out_shape=[jax.Sha...  35.1 us
    unnamed x23, local copies, waits for them, and re-layouts  4.52 us
    reduce_sum x3, other arithmetic, rms_scale(): jnp.mean(widened * widened, -1, keepdims=True) + EPS  3.05 us
    convert_element_type x2, other arithmetic, rms_scale(): return (normed * gain_vec).astype(jnp.bfloat16)  1.88 us

profile of v3, /device:TPU:0, one launch (start us, length us, event | category | flops | bytes accessed | tf_op | source)
XLA Modules:
  0.0 90.9 jit_solution(6616720258251912283)
XLA Ops:
  0.6 0.0 copy-start
  0.7 1.1 %fusion.13 = f32[128]{0:T(128)S(1)} fusion(bf16[128,768]{1,0:T(8,128)(2,1)} %param.19), kind=kLoop, calls=%fused_computation.20 | loop fusion | flops 294784 | bytes 197120 | tf_op jit(solution)/shard_map/reduce_sum | solution.py:22
  1.8 0.9 fusion.28
  2.7 1.0 %fusion.16 = f32[32]{0:T(128)S(1)} fusion(bf16[128,2048]{1,0:T(8,128)(2,1)} %param.28, s32[]{:T(128)S(6)} %select_n.17), kind=kLoop, calls=%fused_computation.25 | loop fusion | flops 196576 | bytes 131204 | tf_op jit(solution)/shard_map/reduce_sum | solution.py:22
  3.8 0.8 constant_dynamic-slice_fusion.1
  4.5 0.8 constant_dynamic-slice_fusion
  5.3 0.1 copy.42
  5.4 0.8 constant_dynamic-slice_fusion.2
  6.2 0.1 copy.46
  6.3 0.1 fusion.38
  6.4 0.0 copy-start.9
  6.4 0.1 copy.41
  6.5 0.1 multiply_cosine_fusion.1
  6.6 0.9 fusion.30
  7.5 0.1 concatenate.13.refs_0_
  7.6 1.0 %fusion.18.refs_1_ = bf16[32,2048]{1,0:T(8,128)(2,1)S(1)} fusion(f32[2048]{0:T(1024)} %param.29, f32[32]{0:T(128)S(1)} %add_rsqrt_fusion.1, bf16[128,2048]{1,0:T(8,128)(2,1)} %param.28, s32[]{:T(128)S(6)} %select_n.17), kind=kLoop, calls=%fused_computation.27 | loop fusion | flops 262144 | bytes 270468 | tf_op jit(solution)/shard_map/convert_element_type | solution.py:23
  8.6 1.6 %fusion.19 = f32[128,384]{0,1:T(8,128)S(1)} fusion(bf16[768,384]{1,0:T(8,128)(2,1)} %param.24, bf16[128,768]{1,0:T(8,128)(2,1)} %param.19, f32[768]{0:T(1024)} %param.22, f32[128]{0:T(128)S(1)} %add_rsqrt_fusion), kind=kOutput, calls=%fused_computation.28 | convolution fusion | flops 75890688 | bytes 986624 | tf_op jit(solution)/shard_map/dot_general | solution.py:700
  10.3 35.1 %shard_map.194 = (bf16[1024,640]{1,0:T(8,128)(2,1)S(1)}, bf16[1024,2048]{1,0:T(8,128)(2,1)S(1)}) custom-call(bf16[32,640]{1,0:T(8,128)(2,1)S(1)} %concatenate.13.refs_0_, bf16[32,2048]{1,0:T(8,128)(2,1)S(1)} %fusion.18.refs_1_), custom_call_target="tpu_custom_call" | custom-call | tf_op jit(solution)/shard_map/pallas_call | solution.py:382
  45.4 0.0 copy-start.1
  45.4 1.9 %copy-done.1 = bf16[1024,2048]{1,0:T(8,128)(2,1)} copy-done((bf16[1024,2048]{1,0:T(8,128)(2,1)}, bf16[1024,2048]{1,0:T(8,128)(2,1)S(1)}, u32[]{:S(2)}) %copy-start.1) | copy-done | bytes 4194328
  47.4 0.1 copy.44
  47.5 0.2 convert_add_fusion.scale_ref
  47.7 0.0 copy-done.9
  47.7 0.8 convolution_convert_fusion.1
  48.5 0.6 multiply_reduce_fusion
  49.1 0.0 copy-start.7
  49.1 0.5 fusion
  49.6 0.0 copy-start.2
  49.6 0.0 copy-start.3
  49.6 0.0 copy-start.4
  49.7 0.0 copy-start.5
  49.7 0.0 copy-start.6
  49.7 0.0 copy-start.8
  49.7 0.6 fusion.3
  50.3 0.0 copy-done
  50.3 0.3 convolution_convert_fusion.head_ref
  50.6 0.0 copy-done.7
  50.7 0.2 copy-done.2
  50.9 0.3 copy-done.3
  51.2 0.3 copy-done.4
  51.5 0.1 copy-done.5
  51.7 0.2 copy-done.6
  51.8 0.0 copy-done.8
  51.8 37.7 %shard_map.195 = (bf16[32,2048]{1,0:T(8,128)(2,1)S(1)}, bf16[128,512]{1,0:T(8,128)(2,1)S(1)}) custom-call(bf16[1024,2048]{1,0:T(8,128)(2,1)} %copy-done.1, f32[1024,1]{1,0:T(8,128)S(1)} %convert_add_fusion.scale_ref, bf16[2048,256]{1,0:T(8,128)(2,1)S(1)} %bitcast.18, bf16[2048,256]{1,0:T(8,128)(2,1)S(1)} %bitcast.19, bf16[256,2048]{1,0:T(8,128)(2,1)S(1)} %bitcast.20, ...), custom_call_target="tpu_custom_call" | custom-call | tf_op jit(solution)/shard_map/pallas_call | solution.py:611
  89.6 0.7 copy.49
  90.2 0.7 copy.50
  (16 shorter events, 0.2 us)
Async XLA Ops:
  0.6 49.7 %copy-start = (bf16[256,2048]{1,0:T(8,128)(2,1)S(1)}, bf16[256,2048]{1,0:T(8,128)(2,1)}, u32[]{:S(2)}) copy-start(bf16[256,2048]{1,0:T(8,128)(2,1)} %param.26) | copy-start | bytes 3145732
  6.4 41.3 %copy-start.9 = (bf16[512,512]{1,0:T(8,128)(2,1)S(1)}, bf16[512,512]{1,0:T(8,128)(2,1)}, u32[]{:S(2)}) copy-start(bf16[512,512]{1,0:T(8,128)(2,1)} %param.25) | copy-start | bytes 1572868
  45.4 1.9 %copy-start.1 = (bf16[1024,2048]{1,0:T(8,128)(2,1)}, bf16[1024,2048]{1,0:T(8,128)(2,1)S(1)}, u32[]{:S(2)}) copy-start(bf16[1024,2048]{1,0:T(8,128)(2,1)S(1)} %get-tuple-element.4.rows_ref) | copy-start | bytes 12582916
  49.1 1.5 %copy-start.7 = (bf16[128,2048]{1,0:T(8,128)(2,1)S(1)}, bf16[128,2048]{1,0:T(8,128)(2,1)}, u32[]{:S(2)}) copy-start(bf16[128,2048]{1,0:T(8,128)(2,1)} %shared_down_ref.1) | copy-start | bytes 1572868
  49.6 1.3 %copy-start.2 = (bf16[1,2048,256]{2,1,0:T(8,128)(2,1)S(1)}, bf16[1,2048,256]{2,1,0:T(8,128)(2,1)}, u32[]{:S(2)}) copy-start(bf16[1,2048,256]{2,1,0:T(8,128)(2,1)} %param.32) | copy-start | bytes 3145732
  49.6 1.6 %copy-start.3 = (bf16[1,2048,256]{2,1,0:T(8,128)(2,1)S(1)}, bf16[1,2048,256]{2,1,0:T(8,128)(2,1)}, u32[]{:S(2)}) copy-start(bf16[1,2048,256]{2,1,0:T(8,128)(2,1)} %param.33) | copy-start | bytes 3145732
  49.6 1.9 %copy-start.4 = (bf16[1,256,2048]{2,1,0:T(8,128)(2,1)S(1)}, bf16[1,256,2048]{2,1,0:T(8,128)(2,1)}, u32[]{:S(2)}) copy-start(bf16[1,256,2048]{2,1,0:T(8,128)(2,1)} %param.34) | copy-start | bytes 3145732
  49.7 2.0 %copy-start.5 = (bf16[2048,128]{1,0:T(8,128)(2,1)S(1)}, bf16[2048,128]{1,0:T(8,128)(2,1)}, u32[]{:S(2)}) copy-start(bf16[2048,128]{1,0:T(8,128)(2,1)} %shared_gate_ref.1) | copy-start | bytes 1572868
  49.7 2.1 %copy-start.6 = (bf16[2048,128]{1,0:T(8,128)(2,1)S(1)}, bf16[2048,128]{1,0:T(8,128)(2,1)}, u32[]{:S(2)}) copy-start(bf16[2048,128]{1,0:T(8,128)(2,1)} %shared_up_ref.1) | copy-start | bytes 1572868
  49.7 2.1 %copy-start.8 = (f32[2048]{0:T(1024)S(1)}, f32[2048]{0:T(1024)}, u32[]{:S(2)}) copy-start(f32[2048]{0:T(1024)} %param.27) | copy-start | bytes 24580
